TPU v7x, 256 devices: a whole 4x4x8 slice. The times are simulated.
256 devices in a mesh: sp: 32 (over z, y), tp: 8 (over x, core).
Axes of the slice: x: 4, y: 4, z: 8, core: 2. Of those that a mesh axis runs over, the one named last changes fastest.
Arguments:
- frames: bfloat16 [8, 4096, 1024], P('tp', 'sp'), may hold values from -22 to 22
- norm_gain: float32 [1024], replicated, may hold values from 0.5 to 1.5
- conv_value_w: bfloat16 [1024, 512], P(None, 'tp'), may hold values from -0.1875 to 0.1875
- conv_gate_w: bfloat16 [1024, 512], P(None, 'tp'), may hold values from -0.1875 to 0.1875
- conv_taps: bfloat16 [31, 512], P(None, 'tp'), may hold values from -1 to 1
- conv_bias: float32 [512], P('tp'), may hold values from -1.2 to 1.2
- channel_gain: float32 [512], P('tp'), may hold values from 0.5 to 1.5
- channel_shift: float32 [512], P('tp'), may hold values from -1.2 to 1.2
- query_w: bfloat16 [1024, 1024], P(None, 'tp'), may hold values from -0.1875 to 0.1875
- forget_w: bfloat16 [1024, 1024], P(None, 'tp'), may hold values from -0.1875 to 0.1875
- input_w: bfloat16 [1024, 1024], P(None, 'tp'), may hold values from -0.1875 to 0.1875
- gate_w: bfloat16 [1024, 1024], P(None, 'tp'), may hold values from -0.1875 to 0.1875
- memory_rate: float32 [1024], P('tp'), may hold values from 0.5 to 32
- head_gain: float32 [1024], P('tp'), may hold values from 0.5 to 1.5
- conv_out_w: bfloat16 [512, 1024], P('tp'), may hold values from -0.1875 to 0.1875
- rec_out_w: bfloat16 [1024, 1024], P('tp'), may hold values from -0.125 to 0.125
Outputs:
- mixed: bfloat16 [8, 4096, 1024], P('tp', 'sp')
All inputs are finite; a program needn't handle non-finite values.
Results may differ from a plain program's by a relative error of at most 0.015.
The roundings to bfloat16 on the way count: a program that leaves them out, or rounds other values in their place, can miss the bound.
Values may be sent and summed in bfloat16 or wider, within the bound.
A program may use at most 64 MiB of HBM per device.

v0:
```python
import jax
import jax.numpy as jnp
from jax import lax
from jax.sharding import Mesh
from jax.sharding import PartitionSpec as P

D_CONV = 512
HEAD = 128
SP = ("sp_0", "sp_1")


EPS = 1e-06


def from_behind(value, axis, steps):
    count = lax.axis_size(axis)
    leading, last = (max(0, -steps), min(count, count - steps))
    return lax.ppermute(value, axis, [(source, source + steps) for source in range(leading, last)])


def copy_for_each(x, axis):
    copies = jnp.broadcast_to(x, (lax.axis_size(axis), *x.shape))
    return lax.all_to_all(copies, axis, split_axis=0, concat_axis=0, tiled=True)


def taken_together(x, axis):
    everything = copy_for_each(x, axis)
    return jnp.sum(everything, axis=0)


def in_one(arrays, axis):
    ends = [0]
    for a in arrays:
        ends.append(ends[-1] + a.size)
    total = taken_together(jnp.concatenate([a.ravel() for a in arrays]), axis)
    return tuple((total[b:e].reshape(a.shape) for a, b, e in zip(arrays, ends, ends[1:])))


def filled_with(x, identity):
    return jax.tree.map(
        lambda a, e: jnp.broadcast_to(jnp.asarray(e, a.dtype), a.shape), x, identity
    )


def carried_in(x, axes, combine, identity):
    before = start = filled_with(x, identity)
    total = x
    for axis in reversed(axes):
        count, position = (lax.axis_size(axis), lax.axis_index(axis))
        pieces = jax.tree.map(lambda part: lax.all_gather(part, axis), total)
        inside, total = (start, start)
        for k in range(count):
            passed = k < position
            total = combine(total, jax.tree.map(lambda part: part[k], pieces))
            inside = jax.tree.map(lambda new, old: jnp.where(passed, new, old), total, inside)
        before = combine(inside, before)
    return before


def in_order(pieces, dim):
    lengths = list(pieces.shape[1:])
    lengths[dim] *= pieces.shape[0]
    return jnp.moveaxis(pieces, 0, dim).reshape(lengths)


def gathered_copies(x, axis, dim):
    return in_order(copy_for_each(x, axis), dim)


def in_blocks(x, dim, count):
    lengths = x.shape
    pieces = x.reshape(*lengths[:dim], count, lengths[dim] // count, *lengths[dim + 1 :])
    return jnp.moveaxis(pieces, dim, 0)


def sent_and_summed(x, axis, dim):
    count = lax.axis_size(axis)
    pieces = lax.all_to_all(in_blocks(x, dim, count), axis, 0, 0, tiled=True)
    return jnp.sum(pieces.astype(jnp.float32), axis=0)


def conv_branch(conv_value, conv_gate, conv_taps, conv_bias, channel_gain, channel_shift):
    gated_conv = (
        conv_value.astype(jnp.float32) * jax.nn.sigmoid(conv_gate.astype(jnp.float32))
    ).astype(jnp.bfloat16)
    positions = gated_conv.shape[1]
    reach_rows = conv_taps.shape[0] - 1
    edge_rows = from_behind(gated_conv[:, positions - reach_rows :, :], SP, 1)
    extended = jnp.concatenate([edge_rows, gated_conv], axis=1)
    filtered = (
        lax.conv_general_dilated(
            extended,
            conv_taps[:, None, :],
            window_strides=(1,),
            padding=[(0, 0)],
            dimension_numbers=("NWC", "WIO", "NWC"),
            feature_group_count=gated_conv.shape[2],
            preferred_element_type=jnp.float32,
        )
        + conv_bias
    )
    row_sums, row_squares = in_one(
        (jnp.sum(filtered, axis=-1), jnp.sum(filtered * filtered, axis=-1)), "tp"
    )
    row_mean = (row_sums / D_CONV)[..., None]
    row_var = (row_squares / D_CONV)[..., None] - row_mean * row_mean
    scaled = (filtered - row_mean) * lax.rsqrt(row_var + EPS) * channel_gain + channel_shift
    return jax.nn.silu(scaled).astype(jnp.bfloat16)


def combine_states(earlier, later):
    return (earlier[0] * later[0], later[0][..., None] * earlier[1] + later[1])


def rec_begin(queries, forget_raw, inputs, memory_rate, seq_total):
    seq_count, positions, rec_local = queries.shape
    head_shape = (seq_count, positions, rec_local // HEAD, HEAD)
    rate_rows = (memory_rate / seq_total).reshape(head_shape[2:])
    in_gate = rate_rows * jax.nn.sigmoid(-forget_raw.astype(jnp.float32)).reshape(head_shape)
    cumulative = jnp.cumsum(jnp.log1p(-in_gate), axis=1)
    final_sum = cumulative[:, -1]
    grown = (queries.astype(jnp.float32).reshape(head_shape) * jnp.exp(cumulative)).astype(
        jnp.bfloat16
    )
    shrunk = (in_gate * jnp.exp(-cumulative)).astype(jnp.bfloat16)
    weighted = (in_gate * jnp.exp(final_sum[:, None] - cumulative)).astype(jnp.bfloat16)
    value_rows = inputs.reshape(head_shape)
    causal = jnp.tril(jnp.ones((positions, positions), dtype=bool))
    scores = jnp.einsum("sthk,suhk->shtu", grown, shrunk, preferred_element_type=jnp.float32)
    scores = jnp.where(causal, scores, 0.0).astype(jnp.bfloat16)
    local_out = jnp.einsum(
        "shtu,suhv->sthv", scores, value_rows, preferred_element_type=jnp.float32
    )
    block_decay = jnp.exp(final_sum)
    block_state = jnp.einsum(
        "suhk,suhv->shkv", weighted, value_rows, preferred_element_type=jnp.float32
    )
    identity = (jnp.ones_like(block_decay), jnp.zeros_like(block_state))
    carried = carried_in((block_decay, block_state), SP, combine_states, identity)
    return (grown, local_out, carried[1])


def rec_finish(grown, local_out, carried_state, out_gate, head_gain):
    carried_low = carried_state.astype(jnp.bfloat16)
    rec_raw = local_out + jnp.einsum(
        "sthk,shkv->sthv", grown, carried_low, preferred_element_type=jnp.float32
    )
    rec_norm = (
        rec_raw
        * lax.rsqrt(jnp.mean(rec_raw * rec_raw, axis=-1, keepdims=True) + EPS)
        * head_gain.reshape(rec_raw.shape[2:])
    )
    return (rec_norm.reshape(out_gate.shape) * jax.nn.silu(out_gate.astype(jnp.float32))).astype(
        jnp.bfloat16
    )


def out_term(branch, weight, row_count):
    rows = lax.slice_in_dim(branch, 0, row_count, axis=0)
    return jnp.einsum("spc,cd->spd", rows, weight, preferred_element_type=jnp.float32)


def local(
    frames,
    norm_gain,
    conv_value_w,
    conv_gate_w,
    conv_taps,
    conv_bias,
    channel_gain,
    channel_shift,
    query_w,
    forget_w,
    input_w,
    gate_w,
    memory_rate,
    head_gain,
    conv_out_w,
    rec_out_w,
):
    values = frames.astype(jnp.float32)
    normed = (
        values * lax.rsqrt(jnp.mean(values * values, axis=-1, keepdims=True) + EPS) * norm_gain
    ).astype(jnp.bfloat16)
    conv_local = conv_value_w.shape[1]
    rec_local = query_w.shape[1]
    joined_weight = jnp.concatenate(
        [conv_value_w, conv_gate_w, query_w, forget_w, input_w, gate_w], axis=1
    )
    product = jnp.einsum(
        "spd,dc->spc",
        gathered_copies(normed, "tp", 0),
        joined_weight,
        preferred_element_type=jnp.float32,
    )
    projected = product.astype(jnp.bfloat16)
    split_points = [
        conv_local,
        2 * conv_local,
        2 * conv_local + rec_local,
        2 * conv_local + 2 * rec_local,
        2 * conv_local + 3 * rec_local,
    ]
    conv_value, conv_gate, queries, forget_raw, inputs, out_gate = jnp.split(
        projected, split_points, axis=-1
    )
    seq_total = frames.shape[1] * lax.axis_size(SP)
    conv_out = conv_branch(conv_value, conv_gate, conv_taps, conv_bias, channel_gain, channel_shift)
    grown, local_out, carried_state = rec_begin(queries, forget_raw, inputs, memory_rate, seq_total)
    rec_out = rec_finish(grown, local_out, carried_state, out_gate, head_gain)
    seq_local = frames.shape[0]
    conv_sum = sent_and_summed(
        out_term(conv_out, conv_out_w, seq_local * lax.axis_size("tp")).astype(jnp.bfloat16),
        "tp",
        0,
    )
    rec_sum = sent_and_summed(
        out_term(rec_out, rec_out_w, seq_local * lax.axis_size("tp")).astype(jnp.bfloat16), "tp", 0
    )
    mixed = conv_sum + rec_sum
    return mixed.astype(jnp.bfloat16)


def solution(mesh):
    torus = Mesh(mesh.devices.reshape(8, 4, mesh.shape["tp"]), ("sp_0", "sp_1", "tp"))
    in_specs = (
        P("tp", SP, None),
        P(),
        P(None, "tp"),
        P(None, "tp"),
        P(None, "tp"),
        P("tp"),
        P("tp"),
        P("tp"),
        P(None, "tp"),
        P(None, "tp"),
        P(None, "tp"),
        P(None, "tp"),
        P("tp"),
        P("tp"),
        P("tp", None),
        P("tp", None),
    )
    out_specs = P("tp", SP, None)
    return jax.shard_map(local, mesh=torus, in_specs=in_specs, out_specs=out_specs, check_vma=False)
```

profile of v0, /device:TPU:1, one launch (start us, length us, event | category | flops | bytes accessed | tf_op | source)
XLA Modules:
  0.0 217.0 jit_solution(14776515510346934009)
XLA Ops:
  6.5 1.1 fusion.9
  8.8 1.6 broadcast_in_dim.37
  10.4 6.8 %all-to-all-start = ((bf16[8,1,128,1024]{3,2,1,0:T(8,128)(2,1)}), bf16[8,1,128,1024]{3,2,1,0:T(8,128)(2,1)S(1)}, u32[]{:S(2)}, u32[]{:S(2)}) async-start(bf16[8,1,128,1024]{3,2,1,0:T(8,128)(2,1)} %broadcast_in_dim.37), calls=%async_computation | async-start | bytes 4194304 | tf_op jit(solution)/shard_map/all_to_all | solution.py:23
  17.6 4.0 %concatenate.9 = bf16[1024,640]{1,0:T(8,128)(2,1)} concatenate(bf16[1024,64]{1,0:T(8,128)(2,1)S(1)} %copy.119, bf16[1024,64]{1,0:T(8,128)(2,1)S(1)} %copy.120, bf16[1024,128]{1,0:T(8,128)(2,1)S(1)} %copy-done.2, bf16[1024,128]{1,0:T(8,128)(2,1)S(1)} %copy-done.3, bf16[1024,128]{1,0:T(8,128)(2,1)} %param.26, bf16[1024,128]{1,0:T(8,128)(2,1)} %param.27), dimensions={1} | concatenate | bytes 2621440 | tf_op jit(solution)/shard_map/concatenate | solution.py:187
  21.6 21.9 %all-to-all-done = bf16[8,1,128,1024]{3,2,1,0:T(8,128)(2,1)S(1)} async-done(((bf16[8,1,128,1024]{3,2,1,0:T(8,128)(2,1)}), bf16[8,1,128,1024]{3,2,1,0:T(8,128)(2,1)S(1)}, u32[]{:S(2)}, u32[]{:S(2)}) %all-to-all-start) | async-done | bytes 2097184 | tf_op jit(solution)/shard_map/all_to_all | solution.py:23
  43.5 2.9 %fusion.2 = bf16[8,128,640]{1,2,0:T(8,128)(2,1)S(1)} fusion(bf16[8,1,128,1024]{3,2,1,0:T(8,128)(2,1)S(1)} %all-to-all-done, bf16[1024,640]{1,0:T(8,128)(2,1)} %concatenate.9), kind=kOutput, calls=%fused_computation.6 | convolution fusion | flops 1342832640 | bytes 4718592 | tf_op jit(solution)/shard_map/spd,dc->spc/dot_general | solution.py:190
  46.4 1.1 copy-done.1
  48.1 23.3 %fusion.86 = f32[8,128,1,128]{3,0,1,2:T(8,128)S(1)} fusion(f32[8,128,1,128]{3,0,1,2:T(8,128)S(1)} %copy.127), kind=kOutput, calls=%fused_computation.134 | output fusion | flops 16646144 | bytes 1048576 | tf_op jit(solution)/shard_map/jit(cumsum)/reduce_window_sum | solution.py:120
  71.6 2.2 %fusion.43 = f32[8,128,128]{2,1,0:T(8,128)} fusion(f32[8,128,1,128]{1,3,0,2:T(8,128)S(1)} %copy.128, f32[8,128]{1,0:T(8,128)S(1)} %get-tuple-element.8, bf16[8,128,640]{1,2,0:T(8,128)(2,1)} %copy-done.1, f32[128]{0:T(128)S(1)} %broadcast_multiply_fusion), kind=kOutput, calls=%fused_computation.69 | convolution fusion | flops 34471936 | bytes 1577472 | tf_op jit(solution)/shard_map/suhk,suhv->shkv/dot_general | solution.py:135
  73.9 9.1 %all-gather = f32[32,1,1,128]{3,0,1,2:T(8,128)S(1)} all-gather(f32[8,1,1,128]{3,0,1,2:T(8,128)S(1)} %get-tuple-element.7), channel_id=2, replica_groups=mesh['sp_0'=8,'sp_1'=4,'tp'=8] {'sp_1'}, dimensions={0}, use_global_device_ids=true | all-gather | bytes 20480 | tf_op jit(solution)/shard_map/all_gather | solution.py:50
  83.1 24.6 %all-gather.7.cloned.1.call-done = f32[32,128,128]{2,1,0:T(8,128)} async-done(((f32[8,128,128]{2,1,0:T(8,128)}), f32[32,128,128]{2,1,0:T(8,128)}) %all-gather.7.cloned.1.call-update) | async-done | bytes 2097168 | tf_op jit(solution)/shard_map/all_gather | solution.py:50
  107.7 2.6 %fusion.28 = f32[1,8,1,128,128]{4,3,2,1,0:T(8,128)} fusion(f32[32,128,128]{2,1,0:T(8,128)} %all-gather.7.cloned.1.call-done, f32[8,128]{1,0:T(8,128)S(1)} %get-tuple-element.18, f32[8,128]{1,0:T(8,128)S(1)} %get-tuple-element.21, f32[8,128]{1,0:T(8,128)S(1)} %slice_bitcast_fusion.16, f32[8,128]{1,0:T(8,128)S(1)} %get-tuple-element.20), kind=kLoop, calls=%fused_computation.45 | loop fusion | flops 917504 | bytes 2637824 | tf_op jit(solution)/shard_map/add | solution.py:112
  111.5 2.1 collective-permute-start
  113.6 1.9 collective-permute-done
  117.5 10.7 %all_to_all.21 = f32[8,1,2048]{2,1,0:T(1,128)S(1)} all-to-all(f32[8,1,2048]{2,1,0:T(1,128)S(1)} %broadcast_in_dim.39), channel_id=1, replica_groups=mesh['sp_0'=8,'sp_1'=4,'tp'=8] {'tp'}, dimensions={0} | all-to-all | bytes 131072 | tf_op jit(solution)/shard_map/all_to_all | solution.py:23
  128.3 2.2 %convert_bitcast_fusion.1 = bf16[8,1,128,1024]{3,2,1,0:T(8,128)(2,1)} fusion(f32[8,128,64]{1,2,0:T(8,128)S(1)} %copy.124, bf16[64,1024]{1,0:T(8,128)(2,1)S(1)} %copy-done.6, f32[64]{0:T(128)S(1)} %copy-done.8, f32[64]{0:T(128)S(1)} %copy-done.9, f32[8,128]{1,0:T(8,128)S(1)} %fusion.75, f32[8,128]{1,0:T(8,128)S(1)} %fusion.76, f32[64]{0:T(128)S(1)} %copy-done.7), kind=kOutput, calls=%fused_computation.5 | convolution fusion | flops 135921664 | bytes 2499328 | tf_op jit(solution)/shard_map/spc,cd->spd/dot_general | solution.py:160
  130.5 4.2 %all-to-all-start.2 = ((bf16[8,1,128,1024]{3,2,1,0:T(8,128)(2,1)}), bf16[8,1,128,1024]{3,2,1,0:T(8,128)(2,1)S(1)}, u32[]{:S(2)}, u32[]{:S(2)}) async-start(bf16[8,1,128,1024]{3,2,1,0:T(8,128)(2,1)} %convert_bitcast_fusion.1), calls=%async_computation.2 | async-start | bytes 4194304 | tf_op jit(solution)/shard_map/all_to_all | solution.py:78
  134.8 28.1 %all_gather.19 = f32[8,8,1,128]{3,1,2,0:T(8,128)S(1)} all-gather(f32[1,8,1,128]{3,1,2,0:T(8,128)S(1)} %get-tuple-element.19), channel_id=1, replica_groups=mesh['sp_0'=8,'sp_1'=4,'tp'=8] {'sp_0'}, dimensions={0}, use_global_device_ids=true | all-gather | bytes 36864 | tf_op jit(solution)/shard_map/all_gather | solution.py:50
  162.8 1.8 fusion.8
  165.6 4.8 %multiply_reduce_fusion = (f32[8,128]{1,0:T(8,128)S(1)}, f32[8,1,128,128]{3,2,0,1:T(8,128)S(1)}) fusion(f32[8,128,128]{2,1,0:T(8,128)S(1)} %fusion.8, f32[8,128,1,128]{1,3,0,2:T(8,128)S(1)} %copy.128, bf16[8,128,640]{1,2,0:T(8,128)(2,1)} %copy-done.1, f32[8,8,1,128,128]{4,3,1,2,0:T(8,128)} %bitcast.249, f32[32,128,128]{2,1,0:T(8,128)} %all-gather.7.cloned.1.call-done, ...), kind=kOutput, calls=%fused_computation.64 | convolution fusion | flops 39189504 | bytes 8183820 | tf_op jit(solution)/shard_map/sthk,shkv->sthv/dot_general | solution.py:145
  170.4 3.1 %convert_bitcast_fusion = bf16[8,1,128,1024]{3,2,1,0:T(8,128)(2,1)} fusion(f32[8,1,128,128]{3,2,0,1:T(8,128)S(1)} %get-tuple-element.23, bf16[8,128,640]{1,2,0:T(8,128)(2,1)} %copy-done.1, bf16[128,1024]{1,0:T(8,128)(2,1)S(1)} %copy-done, f32[128]{0:T(128)S(1)} %copy-done.10, f32[8,128]{1,0:T(8,128)S(1)} %add_rsqrt_fusion), kind=kOutput, calls=%fused_computation.4 | convolution fusion | flops 270663680 | bytes 3150336 | tf_op jit(solution)/shard_map/spc,cd->spd/dot_general | solution.py:160
  173.6 7.5 %all-to-all-start.3 = ((bf16[8,1,128,1024]{3,2,1,0:T(8,128)(2,1)}), bf16[8,1,128,1024]{3,2,1,0:T(8,128)(2,1)}, u32[]{:S(2)}, u32[]{:S(2)}) async-start(bf16[8,1,128,1024]{3,2,1,0:T(8,128)(2,1)} %convert_bitcast_fusion), calls=%async_computation.3 | async-start | bytes 4194304 | tf_op jit(solution)/shard_map/all_to_all | solution.py:78
  181.4 26.0 %all-to-all-done.3 = bf16[8,1,128,1024]{3,2,1,0:T(8,128)(2,1)} async-done(((bf16[8,1,128,1024]{3,2,1,0:T(8,128)(2,1)}), bf16[8,1,128,1024]{3,2,1,0:T(8,128)(2,1)}, u32[]{:S(2)}, u32[]{:S(2)}) %all-to-all-start.3) | async-done | bytes 2097184 | tf_op jit(solution)/shard_map/all_to_all | solution.py:78
  207.4 2.0 convert_reduce_fusion
  (60 shorter events, 7.6 us)
Async XLA Ops:
  6.5 163.9 %copy-start = (bf16[128,1024]{1,0:T(8,128)(2,1)S(1)}, bf16[128,1024]{1,0:T(8,128)(2,1)}, u32[]{:S(2)}) copy-start(bf16[128,1024]{1,0:T(8,128)(2,1)} %param.31) | copy-start | bytes 786436
  10.4 6.9 %copy-start.4 = (bf16[1024,64]{0,1:T(8,128)(2,1)S(1)}, bf16[1024,64]{0,1:T(8,128)(2,1)}, u32[]{:S(2)}) copy-start(bf16[1024,64]{0,1:T(8,128)(2,1)} %param.18) | copy-start | bytes 393220
  10.4 7.0 %copy-start.5 = (bf16[1024,64]{0,1:T(8,128)(2,1)S(1)}, bf16[1024,64]{0,1:T(8,128)(2,1)}, u32[]{:S(2)}) copy-start(bf16[1024,64]{0,1:T(8,128)(2,1)} %param.19) | copy-start | bytes 393220
  10.4 7.2 %copy-start.2 = (bf16[1024,128]{1,0:T(8,128)(2,1)S(1)}, bf16[1024,128]{1,0:T(8,128)(2,1)}, u32[]{:S(2)}) copy-start(bf16[1024,128]{1,0:T(8,128)(2,1)} %param.24) | copy-start | bytes 786436
  10.4 7.2 %copy-start.3 = (bf16[1024,128]{1,0:T(8,128)(2,1)S(1)}, bf16[1024,128]{1,0:T(8,128)(2,1)}, u32[]{:S(2)}) copy-start(bf16[1024,128]{1,0:T(8,128)(2,1)} %param.25) | copy-start | bytes 786436
  10.4 33.1 %all-to-all-start = ((bf16[8,1,128,1024]{3,2,1,0:T(8,128)(2,1)}), bf16[8,1,128,1024]{3,2,1,0:T(8,128)(2,1)S(1)}, u32[]{:S(2)}, u32[]{:S(2)}) async-start(bf16[8,1,128,1024]{3,2,1,0:T(8,128)(2,1)} %broadcast_in_dim.37), calls=%async_computation | async-start | bytes 4194304 | tf_op jit(solution)/shard_map/all_to_all | solution.py:23
  17.2 4.4 %copy-start.12 = (f32[128]{0:T(128)S(1)}, f32[128]{0:T(128)}, u32[]{:S(2)}) copy-start(f32[128]{0:T(128)} %param.28) | copy-start | bytes 1540
  17.2 90.4 %all-gather.7.cloned.1.call-start = ((), (), s32[]{:S(2)}) async-start(), calls=%async_computation.5 | async-start | bytes 2621440 | tf_op jit(solution)/shard_map/all_gather | solution.py:50
  46.4 1.1 copy-start.1
  73.8 91.8 %all-gather.5.cloned.1.call-start = ((), (), s32[]{:S(2)}) async-start(), calls=%async_computation.4 | async-start | bytes 4718592 | tf_op jit(solution)/shard_map/all_gather | solution.py:50
  107.7 8.3 %copy-start.11 = (bf16[31,64]{1,0:T(8,128)(2,1)S(1)}, bf16[31,64]{1,0:T(8,128)(2,1)}, u32[]{:S(2)}) copy-start(bf16[31,64]{1,0:T(8,128)(2,1)} %param.20) | copy-start | bytes 11908
  111.5 4.1 %collective-permute-start = (bf16[8,30,64]{1,2,0:T(8,128)(2,1)S(1)}, bf16[8,30,64]{1,2,0:T(8,128)(2,1)S(1)}, u32[]{:S(2)}, u32[]{:S(2)}) collective-permute-start(bf16[8,30,64]{1,2,0:T(8,128)(2,1)S(1)} %slice.136), channel_id=1, source_target_pairs={{0,8},{8,16},{16,24},{24,32},{32,40},{40,48},{48,56},{56,64},{64,7... | collective-permute-start | bytes 92168 | tf_op jit(solution)/shard_map/ppermute | solution.py:18
  116.0 1.3 copy-start.7
  116.0 12.3 %copy-start.6 = (bf16[64,1024]{1,0:T(8,128)(2,1)S(1)}, bf16[64,1024]{1,0:T(8,128)(2,1)}, u32[]{:S(2)}) copy-start(bf16[64,1024]{1,0:T(8,128)(2,1)} %param.30) | copy-start | bytes 393220
  116.0 12.3 %copy-start.8 = (f32[64]{0:T(128)S(1)}, f32[64]{0:T(128)}, u32[]{:S(2)}) copy-start(f32[64]{0:T(128)} %param.23) | copy-start | bytes 772
  116.0 12.3 %copy-start.9 = (f32[64]{0:T(128)S(1)}, f32[64]{0:T(128)}, u32[]{:S(2)}) copy-start(f32[64]{0:T(128)} %param.22) | copy-start | bytes 772
  130.5 43.1 %all-to-all-start.2 = ((bf16[8,1,128,1024]{3,2,1,0:T(8,128)(2,1)}), bf16[8,1,128,1024]{3,2,1,0:T(8,128)(2,1)S(1)}, u32[]{:S(2)}, u32[]{:S(2)}) async-start(bf16[8,1,128,1024]{3,2,1,0:T(8,128)(2,1)} %convert_bitcast_fusion.1), calls=%async_computation.2 | async-start | bytes 4194304 | tf_op jit(solution)/shard_map/all_to_all | solution.py:78
  165.6 4.8 %copy-start.10 = (f32[128]{0:T(128)S(1)}, f32[128]{0:T(128)}, u32[]{:S(2)}) copy-start(f32[128]{0:T(128)} %param.29) | copy-start | bytes 1540
  173.6 33.8 %all-to-all-start.3 = ((bf16[8,1,128,1024]{3,2,1,0:T(8,128)(2,1)}), bf16[8,1,128,1024]{3,2,1,0:T(8,128)(2,1)}, u32[]{:S(2)}, u32[]{:S(2)}) async-start(bf16[8,1,128,1024]{3,2,1,0:T(8,128)(2,1)} %convert_bitcast_fusion), calls=%async_computation.3 | async-start | bytes 4194304 | tf_op jit(solution)/shard_map/all_to_all | solution.py:78
Sparse Core Ops, SparseCore 0:
  74.0 33.6 all-gather.6
  110.4 55.1 all-gather.4
where the time goes:
time: 218 us; the launch traced here: 217 us
  waiting for transfers between devices  75.4 us (35%)
  blocking collectives  47.9 us (22%)
  other arithmetic  33 us (15%)
  starting transfers between devices  20.7 us (9%)
  matrix products  18 us (8%)
  between operations  13.7 us (6%)
  local copies, waits for them, and re-layouts  8.18 us (4%)
    all_gather x2, blocking collectives, carried_in(): pieces = jax.tree.map(lambda part: lax.all_gather(part, axis), total)  37.2 us
    all_to_all x2, waiting for transfers between devices, sent_and_summed(): pieces = lax.all_to_all(in_blocks(x, dim, count), axis, 0, 0, tiled=True)  26 us
    all_gather x2, waiting for transfers between devices, carried_in(): pieces = jax.tree.map(lambda part: lax.all_gather(part, axis), total)  25.6 us
    another operation x1, other arithmetic, rec_begin(): cumulative = jnp.cumsum(jnp.log1p(-in_gate), axis=1)  23.3 us
    all_to_all x1, waiting for transfers between devices, copy_for_each(): return lax.all_to_all(copies, axis, split_axis=0, concat_axis=0, tiled=True)  21.9 us
    all_to_all x2, starting transfers between devices, sent_and_summed(): pieces = lax.all_to_all(in_blocks(x, dim, count), axis, 0, 0, tiled=True)  11.7 us
    all_to_all x1, blocking collectives, copy_for_each(): return lax.all_to_all(copies, axis, split_axis=0, concat_axis=0, tiled=True)  10.7 us
    all_to_all x1, starting transfers between devices, copy_for_each(): return lax.all_to_all(copies, axis, split_axis=0, concat_axis=0, tiled=True)  6.85 us
  transfers between devices with their start and end apart: 6, of which 5 were waited for; matrix products, arithmetic and copies ran while one was open for 9% of the time, Pallas kernels for 0%

commit v1 on v0

v1 whole, which is shorter than its diff:
```python
import jax
import jax.numpy as jnp
from jax import lax
from jax.experimental import pallas as pl
from jax.experimental.pallas import tpu as pltpu
from jax.sharding import Mesh
from jax.sharding import PartitionSpec as P

F32, BF16 = jnp.float32, jnp.bfloat16
MESH = pl.DeviceIdType.MESH
NZ, NY, NX = 8, 4, 4
EPS = 1e-06
POS, D, HEAD = 128, 1024, 128
TAPS, HALO = 31, 32
D_CONV = 512
SEQ_LEN = 4096
OFF = (0, -1, 1, 2)
SLOT_OF = {0: 0, 3: 1, 1: 2, 2: 3}
FG, IN, QU, GA, CV, CG = 0, 256, 512, 768, 1024, 1152
NT = (((1,), (1,)), ((), ()))
TN = (((0,), (0,)), ((), ()))


def dot(a, b):
    return jnp.dot(a, b, preferred_element_type=F32)


def remote(src, dst, send, recv, dev):
    return pltpu.make_async_remote_copy(
        src_ref=src, dst_ref=dst, send_sem=send, recv_sem=recv, device_id=dev, device_id_type=MESH
    )


def sigmoid(v):
    return 1.0 / (1.0 + jnp.exp(-v))


def kernel(
    frames, norm_gain, cvw, cgw, taps, cbias, cgain, cshift, qw, fw, iw, gw, rate, hgain, cow, row,
    out,
    fr_v, ng_v, taps_v, vec_v, hv_v, pk, xs, w, cvs, wc, wr,
    grown_b, inp_b, shr_b, gate_b, local_b,
    st_s, st_r, dec_s, dec_r, t_s, t_r, dd_s, dd_r, c_s, c_r,
    halo_s, halo_r, ext, filt, stat_s, stat_r, ac_s, ac_r, ar_s, ar_r, out_v,
    lsem, psend, precv, gsend, grecv, r1s, r1r, r2s, r2r, r3s, r3r, hs, hr, ss, sr,
    acs, acr, ars, arr, wxs, wxr, wfs, wfr,
):
    z, y, x, c = (lax.axis_index(a) for a in ("z", "y", "x", "c"))
    partner = {"c": 1 - c}

    def at_x(k):
        return {"x": lax.rem(x + k + NX, NX)}

    def at_y(k):
        return {"y": lax.rem(y + k, NY)}

    bar = pltpu.get_barrier_semaphore()

    def greet(dev):
        pl.semaphore_signal(bar, inc=1, device_id=dev, device_id_type=MESH)

    greet(partner)
    for k in (1, 2, 3):
        greet(at_x(k))
        greet(at_y(k))

    @pl.loop(0, z)
    def _(i):
        greet({"z": i})

    @pl.when((y == 0) & (z > 0))
    def _():
        greet({"z": z - 1, "y": NY - 1})

    loads = []

    def load(src, dst):
        copy = pltpu.make_async_copy(src, dst, lsem.at[len(loads)])
        copy.start()
        loads.append(copy)

    load(frames.at[0], fr_v)
    load(norm_gain, ng_v)
    load(taps, taps_v)
    load(cbias, vec_v.at[0])
    load(cgain, vec_v.at[1])
    load(cshift, vec_v.at[2])
    load(rate, hv_v.at[0])
    load(hgain, hv_v.at[1])
    n_small = len(loads)
    for k, ref in enumerate((fw, iw, qw, gw)):
        load(ref, w.at[:, pl.ds(256 * k, 128)])
    load(cvw, cvs.at[0, 0])
    load(cgw, cvs.at[0, 1])
    load(cow, wc.at[0, pl.ds(0, 64)])
    load(row, wr.at[0, pl.ds(0, 128)])
    for copy in loads[:n_small]:
        copy.wait()

    values = fr_v[...].astype(F32)
    scale = lax.rsqrt(jnp.mean(values * values, axis=-1, keepdims=True) + EPS)
    xs[0] = (values * scale * ng_v[...]).astype(BF16)
    pk[0] = jnp.zeros((40, 128), F32)
    pk[0, 0:TAPS, 0:64] = taps_v[...].astype(F32)
    for k in range(3):
        pk[0, 32 + k : 33 + k, 0:64] = vec_v[k]
    for k in range(2):
        pk[0, 35 + k : 36 + k, :] = hv_v[k]

    pl.semaphore_wait(bar, 7 + (NZ - 1 - z) + jnp.where((y == NY - 1) & (z < NZ - 1), 1, 0))

    def half(ref, s, h):
        return ref.at[s, pl.ds(64 * h, 64)]

    g = [
        remote(half(xs, 0, 0), half(xs, 1, 0), gsend.at[0], grecv.at[0], at_x(1)),
        remote(half(xs, 0, 1), half(xs, 2, 1), gsend.at[1], grecv.at[1], at_x(-1)),
        remote(half(xs, 0, 1), half(xs, 1, 1), gsend.at[2], grecv.at[2], at_x(1)),
        remote(half(xs, 0, 0), half(xs, 2, 0), gsend.at[3], grecv.at[3], at_x(-1)),
        remote(half(xs, 1, 0), half(xs, 3, 0), gsend.at[4], grecv.at[4], at_x(1)),
        remote(half(xs, 2, 1), half(xs, 3, 1), gsend.at[5], grecv.at[5], at_x(-1)),
    ]
    for copy in g[:4]:
        copy.start()

    p = []

    def pair(src, dst):
        copy = remote(src, dst, psend.at[len(p)], precv.at[len(p)], partner)
        copy.start()
        p.append(copy)

    for k, ref in enumerate((fw, iw)):
        pair(ref, w.at[:, pl.ds(256 * k + 128, 128)])
    pair(pk.at[0], pk.at[1])
    for k, ref in enumerate((qw, gw)):
        pair(ref, w.at[:, pl.ds(256 * k + 640, 128)])
    pair(cvw, cvs.at[1, 0])
    pair(cgw, cvs.at[1, 1])
    pair(cow, wc.at[0, pl.ds(64, 64)])
    pair(row, wr.at[0, pl.ds(128, 128)])

    for copy in loads[n_small:]:
        copy.wait()
    for copy in p[:7]:
        copy.wait_recv()

    w[:, CV : CV + 128] = jnp.concatenate([cvs[0, 0], cvs[1, 0]], axis=1)
    w[:, CG : CG + 128] = jnp.concatenate([cvs[0, 1], cvs[1, 1]], axis=1)

    def conv_rows(a, b):
        return jnp.concatenate([pk[0, a:b, 0:64], pk[1, a:b, 0:64]], axis=1)

    tap_rows = conv_rows(0, 32)
    bias_row, gain_row, shift_row = (conv_rows(32 + k, 33 + k) for k in range(3))
    rate_row = jnp.concatenate([pk[0, 35:36], pk[1, 35:36]], axis=1) / SEQ_LEN
    hgain_row = jnp.concatenate([pk[0, 36:37], pk[1, 36:37]], axis=1)

    at_t = lax.broadcasted_iota(jnp.int32, (POS, POS), 0)
    at_u = lax.broadcasted_iota(jnp.int32, (POS, POS), 1)
    causal = at_u <= at_t
    tril = jnp.where(causal, 1.0, 0.0).astype(BF16)

    started = []

    def begin(j):
        rows = xs[j]
        forget_raw = dot(rows, w[:, FG : FG + 256]).astype(BF16).astype(F32)
        inputs = dot(rows, w[:, IN : IN + 256]).astype(BF16)
        in_gate = rate_row * sigmoid(-forget_raw)
        log_forget = jnp.log1p(-in_gate)
        hi = log_forget.astype(BF16)
        rest = log_forget - hi.astype(F32)
        mid = rest.astype(BF16)
        low = (rest - mid.astype(F32)).astype(BF16)
        cumulative = dot(tril, hi) + dot(tril, mid) + dot(tril, low)
        last = cumulative[POS - 1 : POS]
        weighted = (in_gate * jnp.exp(last - cumulative)).astype(BF16)
        for h in range(2):
            lanes = slice(128 * h, 128 * h + 128)
            state = lax.dot_general(
                inputs[:, lanes], weighted[:, lanes], TN, preferred_element_type=F32
            )
            for k in range(NY):
                st_s[j, k, 32 * h : 32 * h + 32] = state[32 * k : 32 * k + 32]
            dec_s[j, h : h + 1] = jnp.exp(last[:, lanes])
        st_r[j, y] = st_s[j, y]
        dec_r[j, y] = dec_s[j]
        for k in (1, 2, 3):
            to = lax.rem(y + k, NY)
            a = remote(st_s.at[j, to], st_r.at[j, y], r1s.at[j, k, 0], r1r.at[j, k, 0], {"y": to})
            b = remote(dec_s.at[j], dec_r.at[j, y], r1s.at[j, k, 1], r1r.at[j, k, 1], {"y": to})
            a.start()
            b.start()
            started.extend((a, b))
        conv_value = dot(rows, w[:, CV : CV + 128]).astype(BF16).astype(F32)
        conv_gate = dot(rows, w[:, CG : CG + 128]).astype(BF16).astype(F32)
        gated = (conv_value * sigmoid(conv_gate)).astype(BF16)
        halo_s[j] = gated[POS - HALO :]
        ext[j, HALO:] = gated.astype(F32)

        @pl.when(y < NY - 1)
        def _():
            remote(halo_s.at[j], halo_r.at[j], hs.at[j], hr.at[j], {"y": y + 1}).start()

        @pl.when((y == NY - 1) & (z < NZ - 1))
        def _():
            remote(halo_s.at[j], halo_r.at[j], hs.at[j], hr.at[j], {"z": z + 1, "y": 0}).start()

        queries = dot(rows, w[:, QU : QU + 256]).astype(BF16).astype(F32)
        grown = (queries * jnp.exp(cumulative)).astype(BF16)
        shrunk = (in_gate * jnp.exp(-cumulative)).astype(BF16)
        grown_b[j] = grown
        for h in range(2):
            lanes = slice(128 * h, 128 * h + 128)
            scores = lax.dot_general(
                grown[:, lanes], shrunk[:, lanes], NT, preferred_element_type=F32
            )
            scores = jnp.where(causal, scores, 0.0).astype(BF16)
            local_b[j, :, lanes] = dot(scores, inputs[:, lanes])
        gate_b[j] = dot(rows, w[:, GA : GA + 256]).astype(BF16)

    def spread(rows2):
        return jnp.concatenate(
            [jnp.broadcast_to(rows2[h : h + 1], (32, 128)) for h in range(2)], axis=0
        )

    def totals(j):
        for k in (1, 2, 3):
            remote(st_s.at[j, 0], st_r.at[j, 0], r1s.at[j, k, 0], r1r.at[j, k, 0], at_y(k)).wait_recv()
            remote(dec_s.at[j], dec_r.at[j, 0], r1s.at[j, k, 1], r1r.at[j, k, 1], at_y(k)).wait_recv()
        total = st_r[j, 0].astype(F32)
        decay = dec_r[j, 0]
        for k in (1, 2, 3):
            total = total * spread(dec_r[j, k]) + st_r[j, k].astype(F32)
            decay = decay * dec_r[j, k]
        t_s[j] = total
        dd_s[j] = decay

        @pl.loop(z + 1, NZ)
        def _(i):
            remote(t_s.at[j], t_r.at[j, z], r2s.at[j, i, 0], r2r.at[j, z, 0], {"z": i}).start()
            remote(dd_s.at[j], dd_r.at[j, z], r2s.at[j, i, 1], r2r.at[j, z, 1], {"z": i}).start()

    def carry(j):
        def step(i, state):
            remote(t_s.at[j], t_r.at[j, i], r2s.at[j, i, 0], r2r.at[j, i, 0], {"z": i}).wait_recv()
            remote(dd_s.at[j], dd_r.at[j, i], r2s.at[j, i, 1], r2r.at[j, i, 1], {"z": i}).wait_recv()
            return state * spread(dd_r[j, i]) + t_r[j, i].astype(F32)

        state = lax.fori_loop(0, z, step, jnp.zeros((64, 128), F32))
        for k in range(NY):
            c_s[j, k] = state.astype(BF16)
            if k < NY - 1:
                state = state * spread(dec_r[j, k]) + st_r[j, k].astype(F32)
        c_r[j, y] = c_s[j, y]
        for k in (1, 2, 3):
            to = lax.rem(y + k, NY)
            a = remote(c_s.at[j, to], c_r.at[j, y], r3s.at[j, k], r3r.at[j, k], {"y": to})
            a.start()
            started.append(a)

    def filtering(j):
        @pl.when((z > 0) | (y > 0))
        def _():
            remote(halo_s.at[j], halo_r.at[j], hs.at[j], hr.at[j], {"y": y}).wait_recv()
            ext[j, 0:HALO] = halo_r[j].astype(F32)

        @pl.when((z == 0) & (y == 0))
        def _():
            ext[j, 0:HALO] = jnp.zeros((HALO, 128), F32)

        acc = jnp.broadcast_to(bias_row, (POS, 128))
        for k in range(TAPS):
            first = HALO - (TAPS - 1) + k
            acc = acc + tap_rows[k : k + 1] * ext[j, first : first + POS]
        filt[j] = acc
        return jnp.sum(acc, axis=-1, keepdims=True), jnp.sum(acc * acc, axis=-1, keepdims=True)

    def conv_norm(j, sums, squares):
        mean = sums / D_CONV
        var = squares / D_CONV - mean * mean
        scaled = (filt[j] - mean) * lax.rsqrt(var + EPS) * gain_row + shift_row
        return (scaled * sigmoid(scaled)).astype(BF16)

    def finish(j):
        for k in (1, 2, 3):
            remote(c_s.at[j, 0], c_r.at[j, 0], r3s.at[j, k], r3r.at[j, k], at_y(k)).wait_recv()
        gate = gate_b[j].astype(F32)
        silu = gate * sigmoid(gate)
        parts = []
        for h in range(2):
            lanes = slice(128 * h, 128 * h + 128)
            low = jnp.concatenate([c_r[j, k, 32 * h : 32 * h + 32] for k in range(NY)], axis=0)
            raw = local_b[j, :, lanes] + lax.dot_general(
                grown_b[j, :, lanes], low, NT, preferred_element_type=F32
            )
            scale = lax.rsqrt(jnp.mean(raw * raw, axis=-1, keepdims=True) + EPS)
            parts.append((raw * scale * hgain_row[:, lanes] * silu[:, lanes]).astype(BF16))
        return jnp.concatenate(parts, axis=1)

    begin(0)
    g[0].wait_recv()
    g[4].start()
    g[1].wait_recv()
    g[5].start()
    wx = []
    for n, k in enumerate((1, -1, 2)):
        s = SLOT_OF[-k % NX]
        a = remote(cow, wc.at[s, pl.ds(0, 64)], wxs.at[0, n], wxr.at[0, n], at_x(k))
        b = remote(row, wr.at[s, pl.ds(0, 128)], wxs.at[1, n], wxr.at[1, n], at_x(k))
        a.start()
        b.start()
        wx.append((s, a, b))
    g[2].wait_recv()
    begin(1)
    totals(0)
    g[3].wait_recv()
    begin(2)
    totals(1)
    carry(0)
    g[4].wait_recv()
    g[5].wait_recv()
    begin(3)
    totals(2)
    carry(1)
    sums = [filtering(j) for j in range(3)]
    totals(3)
    sums.append(filtering(3))
    lane = lax.broadcasted_iota(jnp.int32, (POS, 128), 1)
    packed = jnp.zeros((POS, 128), F32)
    for j in range(4):
        packed = jnp.where(lane == j, sums[j][0], packed)
        packed = jnp.where(lane == 4 + j, sums[j][1], packed)
    stat_s[...] = packed.T[0:8]
    stats = []
    for n, k in enumerate((1, -1, 2)):
        s = SLOT_OF[-k % NX]
        a = remote(stat_s, stat_r.at[s], ss.at[n], sr.at[n], at_x(k))
        a.start()
        stats.append(a)
    carry(2)
    for a in stats:
        a.wait_recv()
    total = stat_s[...]
    sub = lax.broadcasted_iota(jnp.int32, (8, 128), 0)
    for s in (1, 2, 3):
        got = stat_r[s]
        order = [SLOT_OF[(OFF[j] - OFF[s]) % NX] for j in range(4)]
        total = total + jnp.concatenate(
            [got[base + k : base + k + 1] for base in (0, 4) for k in order], axis=0
        )
    columns = jnp.concatenate([total, jnp.zeros((120, 128), F32)], axis=0).T
    actc = []
    for j in range(4):
        rows = conv_norm(j, columns[:, j : j + 1], columns[:, 4 + j : 5 + j])
        if j == 0:
            ac_r[0] = rows
        else:
            ac_s[j] = rows
            a = remote(ac_s.at[j], ac_r.at[SLOT_OF[-OFF[j] % NX]], acs.at[j], acr.at[SLOT_OF[-OFF[j] % NX]], at_x(OFF[j]))
            a.start()
            actc.append(a)
    carry(3)
    wf = []
    for n, (s, a, b) in enumerate(wx):
        a.wait_recv()
        b.wait_recv()
        for m, (ref, size) in enumerate(((wc, 64), (wr, 128))):
            f = remote(ref.at[s, pl.ds(0, size)], ref.at[s, pl.ds(size, size)], wfs.at[m, n], wfr.at[m, n], partner)
            f.start()
            wf.append(f)
    actr = []
    for j in (1, 2, 3, 0):
        rows = finish(j)
        if j == 0:
            ar_r[0] = rows
        else:
            ar_s[j] = rows
            a = remote(ar_s.at[j], ar_r.at[SLOT_OF[-OFF[j] % NX]], ars.at[j], arr.at[SLOT_OF[-OFF[j] % NX]], at_x(OFF[j]))
            a.start()
            actr.append(a)
    for copy in p[7:]:
        copy.wait_recv()
    for f in wf:
        f.wait_recv()
    acc = dot(ac_r[0], wc[0]) + dot(ar_r[0], wr[0])
    for j in (1, 2, 3):
        remote(ac_s.at[j], ac_r.at[j], acs.at[j], acr.at[j], partner).wait_recv()
        acc = acc + dot(ac_r[j], wc[j])
    for j in (1, 2, 3):
        remote(ar_s.at[j], ar_r.at[j], ars.at[j], arr.at[j], partner).wait_recv()
        acc = acc + dot(ar_r[j], wr[j])
    out_v[...] = acc.astype(BF16)
    done = pltpu.make_async_copy(out_v, out.at[0], lsem.at[0])
    done.start()
    for a in g + p + started + stats + actc + actr + wf + [c for t in wx for c in t[1:]]:
        a.wait_send()

    for j in range(4):
        @pl.loop(z + 1, NZ)
        def _(i):
            remote(t_s.at[j], t_r.at[j, z], r2s.at[j, i, 0], r2r.at[j, z, 0], {"z": i}).wait_send()
            remote(dd_s.at[j], dd_r.at[j, z], r2s.at[j, i, 1], r2r.at[j, z, 1], {"z": i}).wait_send()

        @pl.when((y < NY - 1) | (z < NZ - 1))
        def _():
            remote(halo_s.at[j], halo_r.at[j], hs.at[j], hr.at[j], {"y": y}).wait_send()

    done.wait()


def local(
    frames, norm_gain, conv_value_w, conv_gate_w, conv_taps, conv_bias, channel_gain, channel_shift,
    query_w, forget_w, input_w, gate_w, memory_rate, head_gain, conv_out_w, rec_out_w,
):
    dma = pltpu.SemaphoreType.DMA
    scratch = [
        pltpu.VMEM((POS, D), BF16),
        pltpu.VMEM((1, D), F32),
        pltpu.VMEM((TAPS, 64), BF16),
        pltpu.VMEM((3, 1, 64), F32),
        pltpu.VMEM((2, 1, 128), F32),
        pltpu.VMEM((2, 40, 128), F32),
        pltpu.VMEM((4, POS, D), BF16),
        pltpu.VMEM((D, 1280), BF16),
        pltpu.VMEM((2, 2, D, 64), BF16),
        pltpu.VMEM((4, 128, D), BF16),
        pltpu.VMEM((4, 256, D), BF16),
        pltpu.VMEM((4, POS, 256), BF16),
        pltpu.VMEM((4, POS, 256), BF16),
        pltpu.VMEM((4, POS, 256), BF16),
        pltpu.VMEM((4, POS, 256), BF16),
        pltpu.VMEM((4, POS, 256), F32),
        pltpu.VMEM((4, NY, 64, 128), F32),
        pltpu.VMEM((4, NY, 64, 128), F32),
        pltpu.VMEM((4, 2, 128), F32),
        pltpu.VMEM((4, NY, 2, 128), F32),
        pltpu.VMEM((4, 64, 128), F32),
        pltpu.VMEM((4, NZ, 64, 128), F32),
        pltpu.VMEM((4, 2, 128), F32),
        pltpu.VMEM((4, NZ, 2, 128), F32),
        pltpu.VMEM((4, NY, 64, 128), BF16),
        pltpu.VMEM((4, NY, 64, 128), BF16),
        pltpu.VMEM((4, HALO, 128), BF16),
        pltpu.VMEM((4, HALO, 128), BF16),
        pltpu.VMEM((4, HALO + POS, 128), F32),
        pltpu.VMEM((4, POS, 128), F32),
        pltpu.VMEM((8, 128), F32),
        pltpu.VMEM((4, 8, 128), F32),
        pltpu.VMEM((4, POS, 128), BF16),
        pltpu.VMEM((4, POS, 128), BF16),
        pltpu.VMEM((4, POS, 256), BF16),
        pltpu.VMEM((4, POS, 256), BF16),
        pltpu.VMEM((POS, D), BF16),
        dma((16,)),
        dma((9,)), dma((9,)),
        dma((6,)), dma((6,)),
        dma((4, NY, 2)), dma((4, NY, 2)),
        dma((4, NZ, 2)), dma((4, NZ, 2)),
        dma((4, NY)), dma((4, NY)),
        dma((4,)), dma((4,)),
        dma((3,)), dma((3,)),
        dma((4,)), dma((4,)),
        dma((4,)), dma((4,)),
        dma((2, 3)), dma((2, 3)),
        dma((2, 3)), dma((2, 3)),
    ]
    anywhere = pl.BlockSpec(memory_space=pl.ANY)
    return pl.pallas_call(
        kernel,
        out_shape=jax.ShapeDtypeStruct((1, POS, D), BF16),
        in_specs=[anywhere] * 16,
        out_specs=anywhere,
        scratch_shapes=scratch,
        compiler_params=pltpu.CompilerParams(
            collective_id=0, has_side_effects=True, vmem_limit_bytes=48 * 1024 * 1024
        ),
        name="mixer",
    )(
        frames, norm_gain.reshape(1, -1), conv_value_w, conv_gate_w, conv_taps,
        conv_bias.reshape(1, -1), channel_gain.reshape(1, -1), channel_shift.reshape(1, -1),
        query_w, forget_w, input_w, gate_w, memory_rate.reshape(1, -1), head_gain.reshape(1, -1),
        conv_out_w, rec_out_w,
    )


def solution(mesh):
    torus = Mesh(mesh.devices.reshape(NZ, NY, NX, 2), ("z", "y", "x", "c"))
    tp, sp = ("x", "c"), ("z", "y")
    columns, rows, vector = P(None, tp), P(tp, None), P(tp)
    in_specs = (
        P(tp, sp, None), P(), columns, columns, columns, vector, vector, vector,
        columns, columns, columns, columns, vector, vector, rows, rows,
    )
    return jax.shard_map(
        local, mesh=torus, in_specs=in_specs, out_specs=P(tp, sp, None), check_vma=False
    )
```

time: 218 us -> 63.2 us (0.29)
  the two profiles are of different devices: /device:TPU:1 before, /device:TPU:224 now
where the time goes in v1:
time: 63.2 us; the launch traced here: 62.9 us
  Pallas kernels  53.4 us (84%)
  local copies, waits for them, and re-layouts  9.38 us (15%)
    pallas_call x1, Pallas kernels, local(): pl.pallas_call(kernel, out_shape=jax.ShapeDtypeStruct((1, POS, D), BF16),...  53.4 us
    unnamed x31, local copies, waits for them, and re-layouts  9.38 us

profile of v1, /device:TPU:224, one launch (start us, length us, event | category | flops | bytes accessed | tf_op | source)
XLA Modules:
  0.0 62.9 jit_solution(13648783142508503784)
XLA Ops:
  0.0 0.0 copy-start.7
  0.0 0.0 copy-start.9
  0.0 0.0 copy-start.1
  0.0 0.0 copy-start.2
  0.0 1.1 %copy.17.cvw = bf16[1024,64]{1,0:T(8,128)(2,1)S(1)} copy(bf16[1024,64]{0,1:T(8,128)(2,1)} %param.18) | data formatting | bytes 262144 | tf_op args[2]
  1.2 0.0 copy-start
  1.2 1.1 %copy.18.cgw = bf16[1024,64]{1,0:T(8,128)(2,1)S(1)} copy(bf16[1024,64]{0,1:T(8,128)(2,1)} %param.19) | data formatting | bytes 262144 | tf_op args[3]
  2.3 0.0 copy-done.7
  2.3 0.0 copy-done.9
  2.3 0.0 copy-done.10
  2.3 0.0 copy-done.1
  2.3 0.0 copy-done.2
  2.4 0.0 copy-done
  2.4 0.0 copy-start.3
  2.4 0.9 %copy-done.3 = bf16[1024,128]{1,0:T(8,128)(2,1)S(1)} copy-done((bf16[1024,128]{1,0:T(8,128)(2,1)S(1)}, bf16[1024,128]{1,0:T(8,128)(2,1)}, u32[]{:S(2)}) %copy-start.3) | copy-done | bytes 262168
  3.3 0.9 %copy-done.4 = bf16[1024,128]{1,0:T(8,128)(2,1)S(1)} copy-done((bf16[1024,128]{1,0:T(8,128)(2,1)S(1)}, bf16[1024,128]{1,0:T(8,128)(2,1)}, u32[]{:S(2)}) %copy-start.4) | copy-done | bytes 262168
  4.3 0.9 %copy-done.5 = bf16[128,1024]{1,0:T(8,128)(2,1)S(1)} copy-done((bf16[128,1024]{1,0:T(8,128)(2,1)S(1)}, bf16[128,1024]{1,0:T(8,128)(2,1)}, u32[]{:S(2)}) %copy-start.5) | copy-done | bytes 262168
  5.2 0.9 %copy-done.6 = bf16[64,1024]{1,0:T(8,128)(2,1)S(1)} copy-done((bf16[64,1024]{1,0:T(8,128)(2,1)S(1)}, bf16[64,1024]{1,0:T(8,128)(2,1)}, u32[]{:S(2)}) %copy-start.6) | copy-done | bytes 131096
  6.1 0.7 %copy-done.8 = f32[1024]{0:T(1024)S(1)} copy-done((f32[1024]{0:T(1024)S(1)}, f32[1024]{0:T(1024)}, u32[]{:S(2)}) %copy-start.8) | copy-done | bytes 4120
  6.8 0.7 %copy-done.11 = f32[64]{0:T(128)S(1)} copy-done((f32[64]{0:T(128)S(1)}, f32[64]{0:T(128)}, u32[]{:S(2)}) %copy-start.11) | copy-done | bytes 280
  7.5 0.7 %copy-done.12 = f32[128]{0:T(128)S(1)} copy-done((f32[128]{0:T(128)S(1)}, f32[128]{0:T(128)}, u32[]{:S(2)}) %copy-start.12) | copy-done | bytes 536
  8.1 0.7 %copy-done.13 = f32[128]{0:T(128)S(1)} copy-done((f32[128]{0:T(128)S(1)}, f32[128]{0:T(128)}, u32[]{:S(2)}) %copy-start.13) | copy-done | bytes 536
  8.8 53.4 %mixer.1 = bf16[1,128,1024]{2,1,0:T(8,128)(2,1)S(1)} custom-call(bf16[1,128,1024]{2,1,0:T(8,128)(2,1)S(1)} %copy-done, f32[1,1024]{1,0:T(1,128)S(1)} %bitcast.6, bf16[1024,64]{1,0:T(8,128)(2,1)S(1)} %copy.17.cvw, bf16[1024,64]{1,0:T(8,128)(2,1)S(1)} %copy.18.cgw, bf16[31,64]{1,0:T(8,128)(2,1)S(1)} %copy-done.7, f32[1,64]{1,0:T(1,128)S(1)} %bitcast.7, ...), custom_call_target="tpu_custom_call" | custom-call | tf_op jit(solution)/shard_map/mixer/pallas_call | solution.py:470
  62.2 0.7 %copy.20 = bf16[1,128,1024]{2,1,0:T(8,128)(2,1)} copy(bf16[1,128,1024]{2,1,0:T(8,128)(2,1)S(1)} %mixer.1) | data formatting | bytes 524288
  (8 shorter events, 0.0 us)
Async XLA Ops:
  0.0 2.3 %copy-start.7 = (bf16[31,64]{1,0:T(8,128)(2,1)S(1)}, bf16[31,64]{1,0:T(8,128)(2,1)}, u32[]{:S(2)}) copy-start(bf16[31,64]{1,0:T(8,128)(2,1)} %taps.1) | copy-start | bytes 11908
  0.0 2.3 %copy-start.9 = (f32[64]{0:T(128)S(1)}, f32[64]{0:T(128)}, u32[]{:S(2)}) copy-start(f32[64]{0:T(128)} %param.21) | copy-start | bytes 772
  0.0 2.3 %copy-start.10 = (f32[64]{0:T(128)S(1)}, f32[64]{0:T(128)}, u32[]{:S(2)}) copy-start(f32[64]{0:T(128)} %param.22) | copy-start | bytes 772
  0.0 2.3 %copy-start.1 = (bf16[1024,128]{1,0:T(8,128)(2,1)S(1)}, bf16[1024,128]{1,0:T(8,128)(2,1)}, u32[]{:S(2)}) copy-start(bf16[1024,128]{1,0:T(8,128)(2,1)} %qw.1) | copy-start | bytes 786436
  0.0 2.3 %copy-start.2 = (bf16[1024,128]{1,0:T(8,128)(2,1)S(1)}, bf16[1024,128]{1,0:T(8,128)(2,1)}, u32[]{:S(2)}) copy-start(bf16[1024,128]{1,0:T(8,128)(2,1)} %fw.1) | copy-start | bytes 786436
  1.2 1.2 %copy-start = (bf16[1,128,1024]{2,1,0:T(8,128)(2,1)S(1)}, bf16[1,128,1024]{2,1,0:T(8,128)(2,1)}, u32[]{:S(2)}) copy-start(bf16[1,128,1024]{2,1,0:T(8,128)(2,1)} %frames.1) | copy-start | bytes 786436
  2.4 1.0 %copy-start.3 = (bf16[1024,128]{1,0:T(8,128)(2,1)S(1)}, bf16[1024,128]{1,0:T(8,128)(2,1)}, u32[]{:S(2)}) copy-start(bf16[1024,128]{1,0:T(8,128)(2,1)} %iw.1) | copy-start | bytes 786436
  3.3 0.9 %copy-start.4 = (bf16[1024,128]{1,0:T(8,128)(2,1)S(1)}, bf16[1024,128]{1,0:T(8,128)(2,1)}, u32[]{:S(2)}) copy-start(bf16[1024,128]{1,0:T(8,128)(2,1)} %gw.1) | copy-start | bytes 786436
  4.3 0.9 %copy-start.5 = (bf16[128,1024]{1,0:T(8,128)(2,1)S(1)}, bf16[128,1024]{1,0:T(8,128)(2,1)}, u32[]{:S(2)}) copy-start(bf16[128,1024]{1,0:T(8,128)(2,1)} %row.1) | copy-start | bytes 786436
  5.2 0.9 %copy-start.6 = (bf16[64,1024]{1,0:T(8,128)(2,1)S(1)}, bf16[64,1024]{1,0:T(8,128)(2,1)}, u32[]{:S(2)}) copy-start(bf16[64,1024]{1,0:T(8,128)(2,1)} %cow.1) | copy-start | bytes 393220
  6.1 0.7 %copy-start.8 = (f32[1024]{0:T(1024)S(1)}, f32[1024]{0:T(1024)}, u32[]{:S(2)}) copy-start(f32[1024]{0:T(1024)} %param.17) | copy-start | bytes 12292
  6.8 0.7 %copy-start.11 = (f32[64]{0:T(128)S(1)}, f32[64]{0:T(128)}, u32[]{:S(2)}) copy-start(f32[64]{0:T(128)} %param.23) | copy-start | bytes 772
  7.5 0.7 %copy-start.12 = (f32[128]{0:T(128)S(1)}, f32[128]{0:T(128)}, u32[]{:S(2)}) copy-start(f32[128]{0:T(128)} %param.28) | copy-start | bytes 1540
  8.1 0.7 %copy-start.13 = (f32[128]{0:T(128)S(1)}, f32[128]{0:T(128)}, u32[]{:S(2)}) copy-start(f32[128]{0:T(128)} %param.29) | copy-start | bytes 1540

commit v2 on v1

--- a/solution.py
+++ b/solution.py
@@ -16,7 +16,7 @@
 SEQ_LEN = 4096
 OFF = (0, -1, 1, 2)
 SLOT_OF = {0: 0, 3: 1, 1: 2, 2: 3}
-FG, IN, QU, GA, CV, CG = 0, 256, 512, 768, 1024, 1152
+FG, IN, QU, GA = 0, 256, 512, 768
 NT = (((1,), (1,)), ((), ()))
 TN = (((0,), (0,)), ((), ()))
 
@@ -36,17 +36,18 @@
 
 
 def kernel(
-    frames, norm_gain, cvw, cgw, taps, cbias, cgain, cshift, qw, fw, iw, gw, rate, hgain, cow, row,
+    frames, norm_gain, cvt, cgt, taps, cbias, cgain, cshift, qw, fw, iw, gw, rate, hgain, cow, row,
     out,
-    fr_v, ng_v, taps_v, vec_v, hv_v, pk, xs, w, cvs, wc, wr,
-    grown_b, inp_b, shr_b, gate_b, local_b,
-    st_s, st_r, dec_s, dec_r, t_s, t_r, dd_s, dd_r, c_s, c_r,
+    fr_v, ng_v, taps_v, vec_v, hv_v, pk, xs, w, cwt, wc, wr,
+    grown_b, inp_b, shr_b, gate_b, local_b, gt_b, cum_b,
+    st_s, st_r, dec_s, dec_r, t_s, t_r, dd_s, dd_r, u_r, ud_r, h_s, h_r, c_s, c_r,
     halo_s, halo_r, ext, filt, stat_s, stat_r, ac_s, ac_r, ar_s, ar_r, out_v,
-    lsem, psend, precv, gsend, grecv, r1s, r1r, r2s, r2r, r3s, r3r, hs, hr, ss, sr,
-    acs, acr, ars, arr, wxs, wxr, wfs, wfr,
+    lsem, psend, precv, gsend, grecv, r1s, r1r, r2s, r2r, x2s, x2r, h2s, h2r, r3s, r3r, hs, hr, ss, sr,
+    acs, acr, ars, arr, wxs, wxr, wfs, wfr, y_in, z_in,
 ):
     z, y, x, c = (lax.axis_index(a) for a in ("z", "y", "x", "c"))
     partner = {"c": 1 - c}
+    upper, deep = lax.div(z, 4), lax.rem(z, 4)
 
     def at_x(k):
         return {"x": lax.rem(x + k + NX, NX)}
@@ -54,23 +55,17 @@
     def at_y(k):
         return {"y": lax.rem(y + k, NY)}
 
+    def signal(sem, dev):
+        pl.semaphore_signal(sem, inc=1, device_id=dev, device_id_type=MESH)
+
     bar = pltpu.get_barrier_semaphore()
-
-    def greet(dev):
-        pl.semaphore_signal(bar, inc=1, device_id=dev, device_id_type=MESH)
-
-    greet(partner)
+    signal(bar, partner)
     for k in (1, 2, 3):
-        greet(at_x(k))
-        greet(at_y(k))
-
-    @pl.loop(0, z)
-    def _(i):
-        greet({"z": i})
+        signal(bar, at_x(k))
 
     @pl.when((y == 0) & (z > 0))
     def _():
-        greet({"z": z - 1, "y": NY - 1})
+        signal(bar, {"z": z - 1, "y": NY - 1})
 
     loads = []
 
@@ -90,8 +85,8 @@
     n_small = len(loads)
     for k, ref in enumerate((fw, iw, qw, gw)):
         load(ref, w.at[:, pl.ds(256 * k, 128)])
-    load(cvw, cvs.at[0, 0])
-    load(cgw, cvs.at[0, 1])
+    load(cvt, cwt.at[0, pl.ds(0, 64)])
+    load(cgt, cwt.at[1, pl.ds(0, 64)])
     load(cow, wc.at[0, pl.ds(0, 64)])
     load(row, wr.at[0, pl.ds(0, 128)])
     for copy in loads[:n_small]:
@@ -107,7 +102,21 @@
     for k in range(2):
         pk[0, 35 + k : 36 + k, :] = hv_v[k]
 
-    pl.semaphore_wait(bar, 7 + (NZ - 1 - z) + jnp.where((y == NY - 1) & (z < NZ - 1), 1, 0))
+    pl.semaphore_wait(
+        bar,
+        4
+        + jnp.where(y > 0, 1, 0)
+        + jnp.where(z > 0, 1, 0)
+        + jnp.where((y == NY - 1) & (z < NZ - 1), 1, 0),
+    )
+
+    @pl.when(y < NY - 1)
+    def _():
+        signal(bar, {"y": y + 1})
+
+    @pl.when(z < NZ - 1)
+    def _():
+        signal(bar, {"z": z + 1})
 
     def half(ref, s, h):
         return ref.at[s, pl.ds(64 * h, 64)]
@@ -123,6 +132,14 @@
     for copy in g[:4]:
         copy.start()
 
+    @pl.loop(0, y)
+    def _(i):
+        signal(y_in, {"y": i})
+
+    @pl.loop(0, z)
+    def _(i):
+        signal(z_in, {"z": i})
+
     p = []
 
     def pair(src, dst):
@@ -133,20 +150,17 @@
     for k, ref in enumerate((fw, iw)):
         pair(ref, w.at[:, pl.ds(256 * k + 128, 128)])
     pair(pk.at[0], pk.at[1])
+    pair(cvt, cwt.at[0, pl.ds(64, 64)])
+    pair(cgt, cwt.at[1, pl.ds(64, 64)])
     for k, ref in enumerate((qw, gw)):
         pair(ref, w.at[:, pl.ds(256 * k + 640, 128)])
-    pair(cvw, cvs.at[1, 0])
-    pair(cgw, cvs.at[1, 1])
     pair(cow, wc.at[0, pl.ds(64, 64)])
     pair(row, wr.at[0, pl.ds(128, 128)])
 
     for copy in loads[n_small:]:
         copy.wait()
-    for copy in p[:7]:
+    for copy in p[:3]:
         copy.wait_recv()
-
-    w[:, CV : CV + 128] = jnp.concatenate([cvs[0, 0], cvs[1, 0]], axis=1)
-    w[:, CG : CG + 128] = jnp.concatenate([cvs[0, 1], cvs[1, 1]], axis=1)
 
     def conv_rows(a, b):
         return jnp.concatenate([pk[0, a:b, 0:64], pk[1, a:b, 0:64]], axis=1)
@@ -162,6 +176,11 @@
     tril = jnp.where(causal, 1.0, 0.0).astype(BF16)
 
     started = []
+
+    def spread(rows2):
+        return jnp.concatenate(
+            [jnp.broadcast_to(rows2[h : h + 1], (32, 128)) for h in range(2)], axis=0
+        )
 
     def begin(j):
         rows = xs[j]
@@ -184,8 +203,12 @@
             for k in range(NY):
                 st_s[j, k, 32 * h : 32 * h + 32] = state[32 * k : 32 * k + 32]
             dec_s[j, h : h + 1] = jnp.exp(last[:, lanes])
-        st_r[j, y] = st_s[j, y]
-        dec_r[j, y] = dec_s[j]
+        if j == 0:
+
+            @pl.when(y < NY - 1)
+            def _():
+                pl.semaphore_wait(y_in, NY - 1 - y)
+
         for k in (1, 2, 3):
             to = lax.rem(y + k, NY)
             a = remote(st_s.at[j, to], st_r.at[j, y], r1s.at[j, k, 0], r1r.at[j, k, 0], {"y": to})
@@ -193,8 +216,18 @@
             a.start()
             b.start()
             started.extend((a, b))
-        conv_value = dot(rows, w[:, CV : CV + 128]).astype(BF16).astype(F32)
-        conv_gate = dot(rows, w[:, CG : CG + 128]).astype(BF16).astype(F32)
+        st_r[j, y] = st_s[j, y]
+        dec_r[j, y] = dec_s[j]
+        gt_b[j] = in_gate
+        cum_b[j] = cumulative
+        inp_b[j] = inputs
+
+    def gating(j):
+        rows = xs[j]
+        conv_value = lax.dot_general(rows, cwt[0], NT, preferred_element_type=F32)
+        conv_gate = lax.dot_general(rows, cwt[1], NT, preferred_element_type=F32)
+        conv_value = conv_value.astype(BF16).astype(F32)
+        conv_gate = conv_gate.astype(BF16).astype(F32)
         gated = (conv_value * sigmoid(conv_gate)).astype(BF16)
         halo_s[j] = gated[POS - HALO :]
         ext[j, HALO:] = gated.astype(F32)
@@ -207,9 +240,12 @@
         def _():
             remote(halo_s.at[j], halo_r.at[j], hs.at[j], hr.at[j], {"z": z + 1, "y": 0}).start()
 
+    def within(j):
+        rows = xs[j]
         queries = dot(rows, w[:, QU : QU + 256]).astype(BF16).astype(F32)
+        cumulative = cum_b[j]
         grown = (queries * jnp.exp(cumulative)).astype(BF16)
-        shrunk = (in_gate * jnp.exp(-cumulative)).astype(BF16)
+        shrunk = (gt_b[j] * jnp.exp(-cumulative)).astype(BF16)
         grown_b[j] = grown
         for h in range(2):
             lanes = slice(128 * h, 128 * h + 128)
@@ -217,48 +253,80 @@
                 grown[:, lanes], shrunk[:, lanes], NT, preferred_element_type=F32
             )
             scores = jnp.where(causal, scores, 0.0).astype(BF16)
-            local_b[j, :, lanes] = dot(scores, inputs[:, lanes])
+            local_b[j, :, lanes] = dot(scores, inp_b[j, :, lanes])
         gate_b[j] = dot(rows, w[:, GA : GA + 256]).astype(BF16)
-
-    def spread(rows2):
-        return jnp.concatenate(
-            [jnp.broadcast_to(rows2[h : h + 1], (32, 128)) for h in range(2)], axis=0
-        )
 
     def totals(j):
         for k in (1, 2, 3):
             remote(st_s.at[j, 0], st_r.at[j, 0], r1s.at[j, k, 0], r1r.at[j, k, 0], at_y(k)).wait_recv()
             remote(dec_s.at[j], dec_r.at[j, 0], r1s.at[j, k, 1], r1r.at[j, k, 1], at_y(k)).wait_recv()
-        total = st_r[j, 0].astype(F32)
+        total = st_r[j, 0]
         decay = dec_r[j, 0]
         for k in (1, 2, 3):
-            total = total * spread(dec_r[j, k]) + st_r[j, k].astype(F32)
+            total = total * spread(dec_r[j, k]) + st_r[j, k]
             decay = decay * dec_r[j, k]
-        t_s[j] = total
+        t_s[j] = total.reshape(4, 16, 128)
         dd_s[j] = decay
-
-        @pl.loop(z + 1, NZ)
+        if j == 0:
+
+            @pl.when(z < NZ - 1)
+            def _():
+                pl.semaphore_wait(z_in, NZ - 1 - z)
+
+        @pl.loop(deep + 1, 4)
         def _(i):
-            remote(t_s.at[j], t_r.at[j, z], r2s.at[j, i, 0], r2r.at[j, z, 0], {"z": i}).start()
-            remote(dd_s.at[j], dd_r.at[j, z], r2s.at[j, i, 1], r2r.at[j, z, 1], {"z": i}).start()
+            remote(t_s.at[j], t_r.at[j, deep], r2s.at[j, i, 0], r2r.at[j, deep, 0], {"z": 4 * upper + i}).start()
+            remote(dd_s.at[j], dd_r.at[j, deep], r2s.at[j, i, 1], r2r.at[j, deep, 1], {"z": 4 * upper + i}).start()
+
+        @pl.when(upper == 0)
+        def _():
+            @pl.loop(0, 4)
+            def _(i):
+                remote(t_s.at[j, i], u_r.at[j, deep], x2s.at[j, i, 0], x2r.at[j, deep, 0], {"z": 4 + i}).start()
+                remote(dd_s.at[j], ud_r.at[j, deep], x2s.at[j, i, 1], x2r.at[j, deep, 1], {"z": 4 + i}).start()
+
+    def cross(j):
+        @pl.when(upper == 1)
+        def _():
+            first = lax.div(deep, 2)
+            for i in range(4):
+                remote(t_s.at[j, 0], u_r.at[j, i], x2s.at[j, i, 0], x2r.at[j, i, 0], {"z": i}).wait_recv()
+                remote(dd_s.at[j], ud_r.at[j, i], x2s.at[j, i, 1], x2r.at[j, i, 1], {"z": i}).wait_recv()
+            state = u_r[j, 0]
+            for i in range(1, 4):
+                state = state * ud_r[j, i, pl.ds(first, 1)] + u_r[j, i]
+            h_s[j] = state
+            for k in (1, 2, 3):
+                to = lax.rem(deep + k, 4)
+                remote(h_s.at[j], h_r.at[j, deep], h2s.at[j, k], h2r.at[j, k], {"z": 4 + to}).start()
+            h_r[j, deep] = h_s[j]
 
     def carry(j):
+        @pl.when(upper == 0)
+        def _():
+            h_r[j] = jnp.zeros((4, 16, 128), F32)
+
+        @pl.when(upper == 1)
+        def _():
+            for k in (1, 2, 3):
+                remote(h_s.at[j], h_r.at[j, 0], h2s.at[j, k], h2r.at[j, k], {"z": z}).wait_recv()
+
         def step(i, state):
             remote(t_s.at[j], t_r.at[j, i], r2s.at[j, i, 0], r2r.at[j, i, 0], {"z": i}).wait_recv()
             remote(dd_s.at[j], dd_r.at[j, i], r2s.at[j, i, 1], r2r.at[j, i, 1], {"z": i}).wait_recv()
-            return state * spread(dd_r[j, i]) + t_r[j, i].astype(F32)
-
-        state = lax.fori_loop(0, z, step, jnp.zeros((64, 128), F32))
+            return state * spread(dd_r[j, i]) + t_r[j, i].reshape(64, 128)
+
+        state = lax.fori_loop(0, deep, step, h_r[j].reshape(64, 128))
         for k in range(NY):
             c_s[j, k] = state.astype(BF16)
             if k < NY - 1:
-                state = state * spread(dec_r[j, k]) + st_r[j, k].astype(F32)
-        c_r[j, y] = c_s[j, y]
+                state = state * spread(dec_r[j, k]) + st_r[j, k]
         for k in (1, 2, 3):
             to = lax.rem(y + k, NY)
             a = remote(c_s.at[j, to], c_r.at[j, y], r3s.at[j, k], r3r.at[j, k], {"y": to})
             a.start()
             started.append(a)
+        c_r[j, y] = c_s[j, y]
 
     def filtering(j):
         @pl.when((z > 0) | (y > 0))
@@ -299,34 +367,66 @@
             parts.append((raw * scale * hgain_row[:, lanes] * silu[:, lanes]).astype(BF16))
         return jnp.concatenate(parts, axis=1)
 
+    def rec_half(s, h):
+        return wr.at[s, pl.ds(64 * h, 64)]
+
+    def conv_half(s, h):
+        return wc.at[s, pl.ds(32 * h, 32)]
+
+    def own_rec(h):
+        return row.at[pl.ds(64 * h, 64)]
+
+    wx = [
+        remote(own_rec(0), rec_half(1, 0), wxs.at[0], wxr.at[0], at_x(1)),
+        remote(own_rec(1), rec_half(2, 1), wxs.at[1], wxr.at[1], at_x(-1)),
+        remote(own_rec(1), rec_half(1, 1), wxs.at[2], wxr.at[2], at_x(1)),
+        remote(own_rec(0), rec_half(2, 0), wxs.at[3], wxr.at[3], at_x(-1)),
+        remote(rec_half(1, 0), rec_half(3, 0), wxs.at[4], wxr.at[4], at_x(1)),
+        remote(rec_half(2, 1), rec_half(3, 1), wxs.at[5], wxr.at[5], at_x(-1)),
+        remote(cow, wc.at[1, pl.ds(0, 64)], wxs.at[6], wxr.at[6], at_x(1)),
+        remote(cow, wc.at[2, pl.ds(0, 64)], wxs.at[7], wxr.at[7], at_x(-1)),
+        remote(conv_half(1, 0), conv_half(3, 0), wxs.at[8], wxr.at[8], at_x(1)),
+        remote(conv_half(2, 1), conv_half(3, 1), wxs.at[9], wxr.at[9], at_x(-1)),
+    ]
+    wf = []
+
+    def over(ref, s, size):
+        n = len(wf)
+        f = remote(ref.at[s, pl.ds(0, size)], ref.at[s, pl.ds(size, size)], wfs.at[n], wfr.at[n], partner)
+        f.start()
+        wf.append(f)
+
     begin(0)
+    for copy in p[3:7]:
+        copy.wait_recv()
+    gating(0)
     g[0].wait_recv()
     g[4].start()
     g[1].wait_recv()
     g[5].start()
-    wx = []
-    for n, k in enumerate((1, -1, 2)):
-        s = SLOT_OF[-k % NX]
-        a = remote(cow, wc.at[s, pl.ds(0, 64)], wxs.at[0, n], wxr.at[0, n], at_x(k))
-        b = remote(row, wr.at[s, pl.ds(0, 128)], wxs.at[1, n], wxr.at[1, n], at_x(k))
-        a.start()
-        b.start()
-        wx.append((s, a, b))
+    for copy in wx[:4]:
+        copy.start()
+    within(0)
     g[2].wait_recv()
     begin(1)
-    totals(0)
     g[3].wait_recv()
     begin(2)
-    totals(1)
-    carry(0)
+    totals(0)
+    cross(0)
+    gating(1)
+    gating(2)
     g[4].wait_recv()
     g[5].wait_recv()
     begin(3)
+    gating(3)
+    within(1)
+    totals(1)
     totals(2)
-    carry(1)
-    sums = [filtering(j) for j in range(3)]
-    totals(3)
-    sums.append(filtering(3))
+    cross(1)
+    cross(2)
+    within(2)
+    carry(0)
+    sums = [filtering(j) for j in range(4)]
     lane = lax.broadcasted_iota(jnp.int32, (POS, 128), 1)
     packed = jnp.zeros((POS, 128), F32)
     for j in range(4):
@@ -339,11 +439,20 @@
         a = remote(stat_s, stat_r.at[s], ss.at[n], sr.at[n], at_x(k))
         a.start()
         stats.append(a)
+    totals(3)
+    cross(3)
+    wx[0].wait_recv()
+    wx[4].start()
+    wx[1].wait_recv()
+    wx[5].start()
+    for copy in wx[6:8]:
+        copy.start()
+    within(3)
+    carry(1)
     carry(2)
     for a in stats:
         a.wait_recv()
     total = stat_s[...]
-    sub = lax.broadcasted_iota(jnp.int32, (8, 128), 0)
     for s in (1, 2, 3):
         got = stat_r[s]
         order = [SLOT_OF[(OFF[j] - OFF[s]) % NX] for j in range(4)]
@@ -358,33 +467,43 @@
             ac_r[0] = rows
         else:
             ac_s[j] = rows
-            a = remote(ac_s.at[j], ac_r.at[SLOT_OF[-OFF[j] % NX]], acs.at[j], acr.at[SLOT_OF[-OFF[j] % NX]], at_x(OFF[j]))
+            to = SLOT_OF[-OFF[j] % NX]
+            a = remote(ac_s.at[j], ac_r.at[to], acs.at[j], acr.at[to], at_x(OFF[j]))
             a.start()
             actc.append(a)
+    wx[2].wait_recv()
+    over(wr, 1, 128)
+    wx[3].wait_recv()
+    over(wr, 2, 128)
     carry(3)
-    wf = []
-    for n, (s, a, b) in enumerate(wx):
-        a.wait_recv()
-        b.wait_recv()
-        for m, (ref, size) in enumerate(((wc, 64), (wr, 128))):
-            f = remote(ref.at[s, pl.ds(0, size)], ref.at[s, pl.ds(size, size)], wfs.at[m, n], wfr.at[m, n], partner)
-            f.start()
-            wf.append(f)
+    wx[6].wait_recv()
+    wx[8].start()
+    wx[7].wait_recv()
+    wx[9].start()
+    over(wc, 1, 64)
+    over(wc, 2, 64)
     actr = []
-    for j in (1, 2, 3, 0):
+    for j in (1, 2, 0, 3):
         rows = finish(j)
         if j == 0:
             ar_r[0] = rows
         else:
             ar_s[j] = rows
-            a = remote(ar_s.at[j], ar_r.at[SLOT_OF[-OFF[j] % NX]], ars.at[j], arr.at[SLOT_OF[-OFF[j] % NX]], at_x(OFF[j]))
+            to = SLOT_OF[-OFF[j] % NX]
+            a = remote(ar_s.at[j], ar_r.at[to], ars.at[j], arr.at[to], at_x(OFF[j]))
             a.start()
             actr.append(a)
+    wx[4].wait_recv()
+    wx[5].wait_recv()
+    over(wr, 3, 128)
+    wx[8].wait_recv()
+    wx[9].wait_recv()
+    over(wc, 3, 64)
     for copy in p[7:]:
         copy.wait_recv()
+    acc = dot(ac_r[0], wc[0]) + dot(ar_r[0], wr[0])
     for f in wf:
         f.wait_recv()
-    acc = dot(ac_r[0], wc[0]) + dot(ar_r[0], wr[0])
     for j in (1, 2, 3):
         remote(ac_s.at[j], ac_r.at[j], acs.at[j], acr.at[j], partner).wait_recv()
         acc = acc + dot(ac_r[j], wc[j])
@@ -394,14 +513,26 @@
     out_v[...] = acc.astype(BF16)
     done = pltpu.make_async_copy(out_v, out.at[0], lsem.at[0])
     done.start()
-    for a in g + p + started + stats + actc + actr + wf + [c for t in wx for c in t[1:]]:
+    for a in g + p + started + stats + actc + actr + wf + wx:
         a.wait_send()
 
     for j in range(4):
-        @pl.loop(z + 1, NZ)
+        @pl.loop(deep + 1, 4)
         def _(i):
-            remote(t_s.at[j], t_r.at[j, z], r2s.at[j, i, 0], r2r.at[j, z, 0], {"z": i}).wait_send()
-            remote(dd_s.at[j], dd_r.at[j, z], r2s.at[j, i, 1], r2r.at[j, z, 1], {"z": i}).wait_send()
+            remote(t_s.at[j], t_r.at[j, deep], r2s.at[j, i, 0], r2r.at[j, deep, 0], {"z": z}).wait_send()
+            remote(dd_s.at[j], dd_r.at[j, deep], r2s.at[j, i, 1], r2r.at[j, deep, 1], {"z": z}).wait_send()
+
+        @pl.when(upper == 0)
+        def _():
+            @pl.loop(0, 4)
+            def _(i):
+                remote(t_s.at[j, i], u_r.at[j, deep], x2s.at[j, i, 0], x2r.at[j, deep, 0], {"z": z}).wait_send()
+                remote(dd_s.at[j], ud_r.at[j, deep], x2s.at[j, i, 1], x2r.at[j, deep, 1], {"z": z}).wait_send()
+
+        @pl.when(upper == 1)
+        def _():
+            for k in (1, 2, 3):
+                remote(h_s.at[j], h_r.at[j, 0], h2s.at[j, k], h2r.at[j, k], {"z": z}).wait_send()
 
         @pl.when((y < NY - 1) | (z < NZ - 1))
         def _():
@@ -423,8 +554,8 @@
         pltpu.VMEM((2, 1, 128), F32),
         pltpu.VMEM((2, 40, 128), F32),
         pltpu.VMEM((4, POS, D), BF16),
-        pltpu.VMEM((D, 1280), BF16),
-        pltpu.VMEM((2, 2, D, 64), BF16),
+        pltpu.VMEM((D, 1024), BF16),
+        pltpu.VMEM((2, 128, D), BF16),
         pltpu.VMEM((4, 128, D), BF16),
         pltpu.VMEM((4, 256, D), BF16),
         pltpu.VMEM((4, POS, 256), BF16),
@@ -432,14 +563,20 @@
         pltpu.VMEM((4, POS, 256), BF16),
         pltpu.VMEM((4, POS, 256), BF16),
         pltpu.VMEM((4, POS, 256), F32),
+        pltpu.VMEM((4, POS, 256), F32),
+        pltpu.VMEM((4, POS, 256), F32),
         pltpu.VMEM((4, NY, 64, 128), F32),
         pltpu.VMEM((4, NY, 64, 128), F32),
         pltpu.VMEM((4, 2, 128), F32),
         pltpu.VMEM((4, NY, 2, 128), F32),
-        pltpu.VMEM((4, 64, 128), F32),
-        pltpu.VMEM((4, NZ, 64, 128), F32),
+        pltpu.VMEM((4, 4, 16, 128), F32),
+        pltpu.VMEM((4, 4, 4, 16, 128), F32),
         pltpu.VMEM((4, 2, 128), F32),
-        pltpu.VMEM((4, NZ, 2, 128), F32),
+        pltpu.VMEM((4, 4, 2, 128), F32),
+        pltpu.VMEM((4, 4, 16, 128), F32),
+        pltpu.VMEM((4, 4, 2, 128), F32),
+        pltpu.VMEM((4, 16, 128), F32),
+        pltpu.VMEM((4, 4, 16, 128), F32),
         pltpu.VMEM((4, NY, 64, 128), BF16),
         pltpu.VMEM((4, NY, 64, 128), BF16),
         pltpu.VMEM((4, HALO, 128), BF16),
@@ -457,16 +594,19 @@
         dma((9,)), dma((9,)),
         dma((6,)), dma((6,)),
         dma((4, NY, 2)), dma((4, NY, 2)),
-        dma((4, NZ, 2)), dma((4, NZ, 2)),
+        dma((4, 4, 2)), dma((4, 4, 2)),
+        dma((4, 4, 2)), dma((4, 4, 2)),
+        dma((4, 4)), dma((4, 4)),
         dma((4, NY)), dma((4, NY)),
         dma((4,)), dma((4,)),
         dma((3,)), dma((3,)),
         dma((4,)), dma((4,)),
         dma((4,)), dma((4,)),
-        dma((2, 3)), dma((2, 3)),
-        dma((2, 3)), dma((2, 3)),
+        dma((10,)), dma((10,)),
+        dma((6,)), dma((6,)),
+        pltpu.SemaphoreType.REGULAR, pltpu.SemaphoreType.REGULAR,
     ]
-    anywhere = pl.BlockSpec(memory_space=pl.ANY)
+    anywhere = pl.BlockSpec(memory_space=pltpu.HBM)
     return pl.pallas_call(
         kernel,
         out_shape=jax.ShapeDtypeStruct((1, POS, D), BF16),
@@ -474,11 +614,11 @@
         out_specs=anywhere,
         scratch_shapes=scratch,
         compiler_params=pltpu.CompilerParams(
-            collective_id=0, has_side_effects=True, vmem_limit_bytes=48 * 1024 * 1024
+            collective_id=0, has_side_effects=True, vmem_limit_bytes=67043328
         ),
         name="mixer",
     )(
-        frames, norm_gain.reshape(1, -1), conv_value_w, conv_gate_w, conv_taps,
+        frames, norm_gain.reshape(1, -1), conv_value_w.T, conv_gate_w.T, conv_taps,
         conv_bias.reshape(1, -1), channel_gain.reshape(1, -1), channel_shift.reshape(1, -1),
         query_w, forget_w, input_w, gate_w, memory_rate.reshape(1, -1), head_gain.reshape(1, -1),
         conv_out_w, rec_out_w,

time: 63.2 us -> 48.2 us (0.76)
  the two profiles are of different devices: /device:TPU:224 before, /device:TPU:155 now
where the time goes in v2:
time: 48.2 us; the launch traced here: 48 us
  Pallas kernels  46.4 us (96%)
  local copies, waits for them, and re-layouts  1.67 us (3%)
    pallas_call x1, Pallas kernels, local(): pl.pallas_call(kernel, out_shape=jax.ShapeDtypeStruct((1, POS, D), BF16),...  46.4 us
    unnamed x1, local copies, waits for them, and re-layouts  1.67 us

profile of v2, /device:TPU:155, one launch (start us, length us, event | category | flops | bytes accessed | tf_op | source)
XLA Modules:
  0.0 48.0 jit_solution(6544598864671470749)
XLA Ops:
  0.0 46.4 %mixer.1 = bf16[1,128,1024]{2,1,0:T(8,128)(2,1)} custom-call(bf16[1,128,1024]{2,1,0:T(8,128)(2,1)} %frames.1, f32[1,1024]{1,0:T(1,128)} %bitcast.10, bf16[64,1024]{1,0:T(8,128)(2,1)} %bitcast.8, bf16[64,1024]{1,0:T(8,128)(2,1)} %bitcast.9, bf16[31,64]{1,0:T(8,128)(2,1)} %taps.1, f32[1,64]{1,0:T(1,128)} %bitcast.11, f32[1,64]{1,0:T(1,128)} %bitcast.12, ...), custom_call_target="tpu_custom_call" | custom-call | tf_op jit(solution)/shard_map/mixer/pallas_call | solution.py:610
  46.4 1.7 %copy.18 = bf16[1,128,1024]{2,1,0:T(8,128)(2,1)} copy(bf16[1,128,1024]{2,1,0:T(8,128)(2,1)} %mixer.1) | data formatting | bytes 524288

commit v3 on v1

v3 whole, which is shorter than its diff:
```python
import jax
import jax.numpy as jnp
from jax import lax
from jax.experimental import pallas as pl
from jax.experimental.pallas import tpu as pltpu
from jax.sharding import Mesh
from jax.sharding import PartitionSpec as P

F32, BF16 = jnp.float32, jnp.bfloat16
MESH = pl.DeviceIdType.MESH
NZ, NY, NX = 8, 4, 4
EPS = 1e-06
POS, D, HEAD = 128, 1024, 128
TAPS, HALO = 31, 32
D_CONV = 512
SEQ_LEN = 4096
OFF = (0, -1, 1, 2)
SLOT_OF = {0: 0, 3: 1, 1: 2, 2: 3}
FG, IN, QU, GA = 0, 256, 512, 768
NT = (((1,), (1,)), ((), ()))
TN = (((0,), (0,)), ((), ()))


def dot(a, b):
    return jnp.dot(a, b, preferred_element_type=F32)


def remote(src, dst, send, recv, dev):
    return pltpu.make_async_remote_copy(
        src_ref=src, dst_ref=dst, send_sem=send, recv_sem=recv, device_id=dev, device_id_type=MESH
    )


def sigmoid(v):
    return 1.0 / (1.0 + jnp.exp(-v))


def kernel(
    frames, norm_gain, cvt, cgt, taps, cbias, cgain, cshift, qw, fw, iw, gw, rate, hgain, cow, row,
    out,
    fr_v, ng_v, taps_v, vec_v, hv_v, pk, xs, w, cwt, wc, wr,
    grown_b, inp_b, gate_b, local_b, gt_b, cum_b,
    st_s, st_r, dec_s, dec_r, t_s, t_r, dd_s, dd_r, u_s, u_r, e_s, e_r, c_s, c_r,
    halo_s, halo_r, ext, filt, stat_s, stat_r, ac_s, ac_r, ar_s, ar_r,
    lsem, psend, precv, gsend, grecv, r1s, r1r, r2s, r2r, x2s, x2r, h2s, h2r, r3s, r3r, hs, hr,
    ss, sr, acs, acr, ars, arr, wxs, wxr, wfs, wfr, y_in, z_in,
):
    z, y, x, c = (lax.axis_index(a) for a in ("z", "y", "x", "c"))
    partner = {"c": 1 - c}
    upper, deep = lax.div(z, 4), lax.rem(z, 4)

    def at_x(k):
        return {"x": lax.rem(x + k + NX, NX)}

    def signal(sem, dev):
        pl.semaphore_signal(sem, inc=1, device_id=dev, device_id_type=MESH)

    def arrived(ref, sem):
        remote(ref, ref, sem, sem, partner).wait_recv()

    def sent(ref, sem):
        remote(ref, ref, sem, sem, partner).wait_send()

    bar = pltpu.get_barrier_semaphore()
    signal(bar, partner)
    for k in (1, 2, 3):
        signal(bar, at_x(k))

    @pl.loop(y + 1, NY)
    def _(i):
        signal(bar, {"y": i})

    @pl.loop(z + 1, NZ)
    def _(i):
        signal(bar, {"z": i})

    @pl.when((y == 0) & (z > 0))
    def _():
        signal(bar, {"z": z - 1, "y": NY - 1})

    loaded = []

    def load(src, dst, n):
        pltpu.make_async_copy(src, dst, lsem.at[n]).start()

    def wait_load(ref, n):
        pltpu.make_async_copy(ref, ref, lsem.at[n]).wait()

    load(frames.at[0], fr_v, 0)
    load(norm_gain, ng_v, 1)
    small = ((taps, taps_v), (cbias, vec_v.at[0]), (cgain, vec_v.at[1]), (cshift, vec_v.at[2]), (rate, hv_v.at[0]), (hgain, hv_v.at[1]))
    for n, (src, dst) in enumerate(small):
        load(src, dst, 2 + n)
    load(fw, w.at[:, pl.ds(FG, 128)], 8)
    load(iw, w.at[:, pl.ds(IN, 128)], 8)
    load(qw, w.at[:, pl.ds(QU, 128)], 9)
    load(gw, w.at[:, pl.ds(GA, 128)], 9)
    load(cvt, cwt.at[0, pl.ds(0, 64)], 10)
    load(cgt, cwt.at[1, pl.ds(0, 64)], 10)
    load(cow, wc.at[0, pl.ds(0, 64)], 11)
    load(row, wr.at[0, pl.ds(0, 128)], 12)
    wait_load(fr_v, 0)
    wait_load(ng_v, 1)

    values = fr_v[...].astype(F32)
    scale = lax.rsqrt(jnp.mean(values * values, axis=-1, keepdims=True) + EPS)
    xs[0] = (values * scale * ng_v[...]).astype(BF16)
    for n, (src, dst) in enumerate(small):
        wait_load(dst, 2 + n)
    pk[0] = jnp.zeros((40, 128), F32)
    pk[0, 0:TAPS, 0:64] = taps_v[...].astype(F32)
    for k in range(3):
        pk[0, 32 + k : 33 + k, 0:64] = vec_v[k]
    for k in range(2):
        pk[0, 35 + k : 36 + k, :] = hv_v[k]

    pl.semaphore_wait(
        bar,
        4 + y + z + jnp.where((y == NY - 1) & (z < NZ - 1), 1, 0),
    )

    def half(ref, s, h):
        return ref.at[s, pl.ds(64 * h, 64)]

    g = [
        remote(half(xs, 0, 0), half(xs, 1, 0), gsend, grecv.at[0], at_x(1)),
        remote(half(xs, 0, 1), half(xs, 2, 1), gsend, grecv.at[1], at_x(-1)),
        remote(half(xs, 0, 1), half(xs, 1, 1), gsend, grecv.at[2], at_x(1)),
        remote(half(xs, 0, 0), half(xs, 2, 0), gsend, grecv.at[3], at_x(-1)),
        remote(half(xs, 1, 0), half(xs, 3, 0), gsend, grecv.at[4], at_x(1)),
        remote(half(xs, 2, 1), half(xs, 3, 1), gsend, grecv.at[5], at_x(-1)),
    ]
    for copy in g[:4]:
        copy.start()

    @pl.loop(0, y)
    def _(i):
        signal(y_in, {"y": i})

    @pl.loop(4 * upper, z)
    def _(i):
        signal(z_in, {"z": i})

    @pl.when(upper == 1)
    def _():
        signal(z_in, {"z": z - 4})

    remote(fw, w.at[:, pl.ds(FG + 128, 128)], psend.at[0], precv.at[0], partner).start()
    remote(iw, w.at[:, pl.ds(IN + 128, 128)], psend.at[0], precv.at[0], partner).start()
    remote(pk.at[0], pk.at[1], psend.at[2], precv.at[3], partner).start()
    remote(cvt, cwt.at[0, pl.ds(64, 64)], psend.at[1], precv.at[2], partner).start()
    remote(cgt, cwt.at[1, pl.ds(64, 64)], psend.at[1], precv.at[2], partner).start()
    remote(qw, w.at[:, pl.ds(QU + 128, 128)], psend.at[0], precv.at[1], partner).start()
    remote(gw, w.at[:, pl.ds(GA + 128, 128)], psend.at[0], precv.at[1], partner).start()
    remote(cow, wc.at[0, pl.ds(64, 64)], psend.at[3], precv.at[4], partner).start()
    remote(row, wr.at[0, pl.ds(128, 128)], psend.at[4], precv.at[5], partner).start()

    wait_load(w.at[:, pl.ds(0, 256)], 8)
    wait_load(w.at[:, pl.ds(0, 256)], 9)
    wait_load(cwt.at[0], 10)
    arrived(w.at[:, pl.ds(0, 256)], precv.at[0])
    arrived(pk.at[1], precv.at[3])

    def conv_rows(a, b):
        return jnp.concatenate([pk[0, a:b, 0:64], pk[1, a:b, 0:64]], axis=1)

    tap_rows = conv_rows(0, 32)
    bias_row, gain_row, shift_row = (conv_rows(32 + k, 33 + k) for k in range(3))
    rate_row = jnp.concatenate([pk[0, 35:36], pk[1, 35:36]], axis=1) / SEQ_LEN
    hgain_row = jnp.concatenate([pk[0, 36:37], pk[1, 36:37]], axis=1)

    at_t = lax.broadcasted_iota(jnp.int32, (POS, POS), 0)
    at_u = lax.broadcasted_iota(jnp.int32, (POS, POS), 1)
    causal = at_u <= at_t
    tril = jnp.where(causal, 1.0, 0.0).astype(BF16)

    def spread(rows2):
        return jnp.concatenate(
            [jnp.broadcast_to(rows2[h : h + 1], (32, 128)) for h in range(2)], axis=0
        )

    def begin(j):
        rows = xs[j]
        forget_raw = dot(rows, w[:, FG : FG + 256]).astype(BF16).astype(F32)
        inputs = dot(rows, w[:, IN : IN + 256]).astype(BF16)
        in_gate = rate_row * sigmoid(-forget_raw)
        log_forget = jnp.log1p(-in_gate)
        hi = log_forget.astype(BF16)
        rest = log_forget - hi.astype(F32)
        mid = rest.astype(BF16)
        low = (rest - mid.astype(F32)).astype(BF16)
        cumulative = dot(tril, hi) + dot(tril, mid) + dot(tril, low)
        last = cumulative[POS - 1 : POS]
        weighted = (in_gate * jnp.exp(last - cumulative)).astype(BF16)
        for h in range(2):
            lanes = slice(128 * h, 128 * h + 128)
            state = lax.dot_general(
                inputs[:, lanes], weighted[:, lanes], TN, preferred_element_type=F32
            )
            for k in range(NY):
                st_s[j, k, 32 * h : 32 * h + 32] = state[32 * k : 32 * k + 32]
            dec_s[j, h : h + 1] = jnp.exp(last[:, lanes])
        gt_b[j] = in_gate
        cum_b[j] = cumulative
        inp_b[j] = inputs

    def deal(j):
        for k in (2, 1, 3):
            to = lax.rem(y + k, NY)
            remote(st_s.at[j, to], st_r.at[j, y], r1s.at[0], r1r.at[j, 0], {"y": to}).start()
            remote(dec_s.at[j], dec_r.at[j, y], r1s.at[1], r1r.at[j, 1], {"y": to}).start()
        st_r[j, y] = st_s[j, y]
        dec_r[j, y] = dec_s[j]

    def gating(j):
        rows = xs[j]
        conv_value = lax.dot_general(rows, cwt[0], NT, preferred_element_type=F32)
        conv_gate = lax.dot_general(rows, cwt[1], NT, preferred_element_type=F32)
        conv_value = conv_value.astype(BF16).astype(F32)
        conv_gate = conv_gate.astype(BF16).astype(F32)
        gated = (conv_value * sigmoid(conv_gate)).astype(BF16)
        halo_s[j] = gated[POS - HALO :]
        ext[j, HALO:] = gated.astype(F32)

    def pass_on(j):
        @pl.when(y < NY - 1)
        def _():
            remote(halo_s.at[j], halo_r.at[j], hs, hr.at[j], {"y": y + 1}).start()

        @pl.when((y == NY - 1) & (z < NZ - 1))
        def _():
            remote(halo_s.at[j], halo_r.at[j], hs, hr.at[j], {"z": z + 1, "y": 0}).start()

    def within(j):
        rows = xs[j]
        queries = dot(rows, w[:, QU : QU + 256]).astype(BF16).astype(F32)
        cumulative = cum_b[j]
        grown = (queries * jnp.exp(cumulative)).astype(BF16)
        shrunk = (gt_b[j] * jnp.exp(-cumulative)).astype(BF16)
        grown_b[j] = grown
        for h in range(2):
            lanes = slice(128 * h, 128 * h + 128)
            scores = lax.dot_general(
                grown[:, lanes], shrunk[:, lanes], NT, preferred_element_type=F32
            )
            scores = jnp.where(causal, scores, 0.0).astype(BF16)
            local_b[j, :, lanes] = dot(scores, inp_b[j, :, lanes])
        gate_b[j] = dot(rows, w[:, GA : GA + 256]).astype(BF16)

    def totals(j):
        arrived(st_r.at[j, pl.ds(0, 3)], r1r.at[j, 0])
        arrived(dec_r.at[j, pl.ds(0, 3)], r1r.at[j, 1])
        total = st_r[j, 0]
        decay = dec_r[j, 0]
        for k in (1, 2, 3):
            total = total * spread(dec_r[j, k]) + st_r[j, k]
            decay = decay * dec_r[j, k]
        t_s[j] = total.reshape(4, 16, 128)
        dd_s[j] = decay
        for k in (2, 1, 3):
            to = lax.rem(deep + k, 4)
            dev = {"z": 4 * upper + to}
            remote(t_s.at[j, to], t_r.at[j, deep], r2s.at[0], r2r.at[j, 0], dev).start()
            remote(dd_s.at[j], dd_r.at[j, deep], r2s.at[1], r2r.at[j, 1], dev).start()
        t_r[j, deep] = t_s[j, deep]
        dd_r[j, deep] = dd_s[j]

    def fold(j):
        head = lax.div(deep, 2)
        arrived(t_r.at[j, pl.ds(0, 3)], r2r.at[j, 0])
        arrived(dd_r.at[j, pl.ds(0, 3)], r2r.at[j, 1])

        @pl.when(upper == 0)
        def _():
            u_r[j] = jnp.zeros((16, 128), F32)

        @pl.when(upper == 1)
        def _():
            arrived(u_r.at[j], x2r.at[j])

        state = u_r[j]
        for i in range(4):
            e_s[j, i] = state
            state = state * dd_r[j, i, pl.ds(head, 1)] + t_r[j, i]
        u_s[j] = state

        @pl.when(upper == 0)
        def _():
            remote(u_s.at[j], u_r.at[j], x2s, x2r.at[j], {"z": z + 4}).start()

        for k in (2, 1, 3):
            to = lax.rem(deep + k, 4)
            remote(e_s.at[j, to], e_r.at[j, deep], h2s, h2r.at[j], {"z": 4 * upper + to}).start()
        e_r[j, deep] = e_s[j, deep]

    def carry(j):
        arrived(e_r.at[j, pl.ds(0, 3)], h2r.at[j])
        state = e_r[j].reshape(64, 128)
        for k in range(NY):
            c_s[j, k] = state.astype(BF16)
            if k < NY - 1:
                state = state * spread(dec_r[j, k]) + st_r[j, k]
        for k in (2, 1, 3):
            to = lax.rem(y + k, NY)
            remote(c_s.at[j, to], c_r.at[j, y], r3s, r3r.at[j], {"y": to}).start()
        c_r[j, y] = c_s[j, y]

    def filtering(j):
        @pl.when((z > 0) | (y > 0))
        def _():
            arrived(halo_r.at[j], hr.at[j])
            ext[j, 0:HALO] = halo_r[j].astype(F32)

        @pl.when((z == 0) & (y == 0))
        def _():
            ext[j, 0:HALO] = jnp.zeros((HALO, 128), F32)

        acc = jnp.broadcast_to(bias_row, (POS, 128))
        for k in range(TAPS):
            first = HALO - (TAPS - 1) + k
            acc = acc + tap_rows[k : k + 1] * ext[j, first : first + POS]
        filt[j] = acc
        return jnp.sum(acc, axis=-1, keepdims=True), jnp.sum(acc * acc, axis=-1, keepdims=True)

    def conv_norm(j, sums, squares):
        mean = sums / D_CONV
        var = squares / D_CONV - mean * mean
        scaled = (filt[j] - mean) * lax.rsqrt(var + EPS) * gain_row + shift_row
        return (scaled * sigmoid(scaled)).astype(BF16)

    def finish(j):
        arrived(c_r.at[j, pl.ds(0, 3)], r3r.at[j])
        gate = gate_b[j].astype(F32)
        silu = gate * sigmoid(gate)
        parts = []
        for h in range(2):
            lanes = slice(128 * h, 128 * h + 128)
            low = jnp.concatenate([c_r[j, k, 32 * h : 32 * h + 32] for k in range(NY)], axis=0)
            raw = local_b[j, :, lanes] + lax.dot_general(
                grown_b[j, :, lanes], low, NT, preferred_element_type=F32
            )
            scale = lax.rsqrt(jnp.mean(raw * raw, axis=-1, keepdims=True) + EPS)
            parts.append((raw * scale * hgain_row[:, lanes] * silu[:, lanes]).astype(BF16))
        return jnp.concatenate(parts, axis=1)

    def rec_half(s, h):
        return wr.at[s, pl.ds(64 * h, 64)]

    def conv_half(s, h):
        return wc.at[s, pl.ds(32 * h, 32)]

    def own(h):
        return row.at[pl.ds(64 * h, 64)], cow.at[pl.ds(32 * h, 32)]

    rs, cs = wxs.at[0], wxs.at[1]

    def send_own(k, h):
        s = SLOT_OF[-k % NX]
        a, b = own(h)
        remote(a, rec_half(s, h), rs, wxr.at[s, h, 0], at_x(k)).start()
        remote(b, conv_half(s, h), cs, wxr.at[s, h, 1], at_x(k)).start()

    def send_on(k, h):
        s = SLOT_OF[-k % NX]
        arrived(rec_half(s, h), wxr.at[s, h, 0])
        remote(rec_half(s, h), rec_half(3, h), rs, wxr.at[3, h, 0], at_x(k)).start()
        arrived(conv_half(s, h), wxr.at[s, h, 1])
        remote(conv_half(s, h), conv_half(3, h), cs, wxr.at[3, h, 1], at_x(k)).start()

    def over(s, halves):
        for h in halves:
            arrived(rec_half(s, h), wxr.at[s, h, 0])
            arrived(conv_half(s, h), wxr.at[s, h, 1])
        remote(wr.at[s, pl.ds(0, 128)], wr.at[s, pl.ds(128, 128)], wfs.at[0], wfr.at[0], partner).start()
        remote(wc.at[s, pl.ds(0, 64)], wc.at[s, pl.ds(64, 64)], wfs.at[1], wfr.at[1], partner).start()

    def spread_out(j, rows):
        if j == 0:
            ar_r[3] = rows
        else:
            ar_s[j - 1] = rows
            to = SLOT_OF[-OFF[j] % NX] - 1
            remote(ar_s.at[j - 1], ar_r.at[to], ars, arr.at[to], at_x(OFF[j])).start()

    begin(0)
    arrived(cwt.at[0], precv.at[2])
    gating(0)

    @pl.when(y < NY - 1)
    def _():
        pl.semaphore_wait(y_in, NY - 1 - y)

    deal(0)
    pass_on(0)
    arrived(w.at[:, pl.ds(0, 256)], precv.at[1])
    within(0)
    g[0].wait_recv()
    g[4].start()
    g[1].wait_recv()
    g[5].start()
    send_own(1, 0)
    send_own(-1, 1)
    send_own(1, 1)
    send_own(-1, 0)
    g[2].wait_recv()
    begin(1)
    deal(1)
    g[3].wait_recv()
    begin(2)
    deal(2)

    @pl.when(z < NZ - 1)
    def _():
        pl.semaphore_wait(z_in, 4 - deep - upper)

    totals(0)
    g[4].wait_recv()
    g[5].wait_recv()
    begin(3)
    deal(3)
    gating(1)
    pass_on(1)
    gating(2)
    pass_on(2)
    gating(3)
    pass_on(3)
    totals(1)
    totals(2)
    fold(0)
    within(1)
    totals(3)
    sums = [filtering(j) for j in range(4)]
    lane = lax.broadcasted_iota(jnp.int32, (POS, 128), 1)
    packed = jnp.zeros((POS, 128), F32)
    for j in range(4):
        packed = jnp.where(lane == j, sums[j][0], packed)
        packed = jnp.where(lane == 4 + j, sums[j][1], packed)
    stat_s[...] = packed.T[0:8]
    for k in (1, -1, 2):
        remote(stat_s, stat_r.at[SLOT_OF[-k % NX] - 1], ss, sr, at_x(k)).start()
    within(2)
    fold(1)
    fold(2)
    send_on(1, 0)
    send_on(-1, 1)
    within(3)
    carry(0)
    fold(3)
    arrived(stat_r, sr)
    total = stat_s[...]
    for s in (1, 2, 3):
        got = stat_r[s - 1]
        order = [SLOT_OF[(OFF[j] - OFF[s]) % NX] for j in range(4)]
        total = total + jnp.concatenate(
            [got[base + k : base + k + 1] for base in (0, 4) for k in order], axis=0
        )
    columns = jnp.concatenate([total, jnp.zeros((120, 128), F32)], axis=0).T
    for j in range(4):
        rows = conv_norm(j, columns[:, j : j + 1], columns[:, 4 + j : 5 + j])
        if j == 0:
            ac_r[3] = rows
        else:
            ac_s[j - 1] = rows
            remote(ac_s.at[j - 1], ac_r.at[SLOT_OF[-OFF[j] % NX] - 1], acs, acr, at_x(OFF[j])).start()
    carry(1)
    carry(2)
    over(1, (1,))
    over(2, (0,))
    carry(3)
    spread_out(0, finish(0))
    for j in (1, 2):
        rows = finish(j)
        spread_out(j, rows)
    over(3, (0, 1))
    rows = finish(3)
    spread_out(3, rows)
    wait_load(wc.at[0, pl.ds(0, 64)], 11)
    wait_load(wr.at[0, pl.ds(0, 128)], 12)
    arrived(wc.at[0, pl.ds(0, 64)], precv.at[4])
    arrived(wr.at[0, pl.ds(0, 128)], precv.at[5])
    acc = dot(ac_r[3], wc[0]) + dot(ar_r[3], wr[0])
    arrived(wc.at[pl.ds(0, 3), pl.ds(0, 64)], wfr.at[1])
    arrived(ac_r.at[pl.ds(0, 3)], acr)
    for j in (1, 2, 3):
        acc = acc + dot(ac_r[j - 1], wc[j])
    arrived(wr.at[pl.ds(0, 3), pl.ds(0, 128)], wfr.at[0])
    for j in (1, 2, 3):
        arrived(ar_r.at[j - 1], arr.at[j - 1])
        acc = acc + dot(ar_r[j - 1], wr[j])
    out[0] = acc.astype(BF16)

    sent(w.at[:, pl.ds(0, 512)], psend.at[0])
    sent(cwt.at[0], psend.at[1])
    sent(pk.at[0], psend.at[2])
    sent(wc.at[0, pl.ds(0, 64)], psend.at[3])
    sent(wr.at[0, pl.ds(0, 128)], psend.at[4])
    sent(xs.at[pl.ds(0, 3)], gsend)
    sent(st_s.at[pl.ds(0, 3)], r1s.at[0])
    sent(dec_r.at[pl.ds(0, 3)], r1s.at[1])
    sent(t_r.at[pl.ds(0, 3)], r2s.at[0])
    sent(dd_r.at[pl.ds(0, 3)], r2s.at[1])
    sent(e_r.at[pl.ds(0, 3)], h2s)

    @pl.when(upper == 0)
    def _():
        sent(u_s, x2s)

    sent(c_r.at[pl.ds(0, 3)], r3s)

    @pl.when((y < NY - 1) | (z < NZ - 1))
    def _():
        sent(halo_s, hs)

    sent(stat_r, ss)
    sent(ac_s, acs)
    sent(ar_s, ars)
    sent(wr.at[pl.ds(0, 3), pl.ds(0, 128)], wxs.at[0])
    sent(wc.at[pl.ds(0, 3), pl.ds(0, 64)], wxs.at[1])
    sent(wr.at[pl.ds(0, 3), pl.ds(0, 128)], wfs.at[0])
    sent(wc.at[pl.ds(0, 3), pl.ds(0, 64)], wfs.at[1])


def local(
    frames, norm_gain, conv_value_w, conv_gate_w, conv_taps, conv_bias, channel_gain, channel_shift,
    query_w, forget_w, input_w, gate_w, memory_rate, head_gain, conv_out_w, rec_out_w,
):
    dma = pltpu.SemaphoreType.DMA
    scratch = [
        pltpu.VMEM((POS, D), BF16),
        pltpu.VMEM((1, D), F32),
        pltpu.VMEM((TAPS, 64), BF16),
        pltpu.VMEM((3, 1, 64), F32),
        pltpu.VMEM((2, 1, 128), F32),
        pltpu.VMEM((2, 40, 128), F32),
        pltpu.VMEM((4, POS, D), BF16),
        pltpu.VMEM((D, 1024), BF16),
        pltpu.VMEM((2, 128, D), BF16),
        pltpu.VMEM((4, 128, D), BF16),
        pltpu.VMEM((4, 256, D), BF16),
        pltpu.VMEM((4, POS, 256), BF16),
        pltpu.VMEM((4, POS, 256), BF16),
        pltpu.VMEM((4, POS, 256), BF16),
        pltpu.VMEM((4, POS, 256), F32),
        pltpu.VMEM((4, POS, 256), F32),
        pltpu.VMEM((4, POS, 256), F32),
        pltpu.VMEM((4, NY, 64, 128), F32),
        pltpu.VMEM((4, NY, 64, 128), F32),
        pltpu.VMEM((4, 2, 128), F32),
        pltpu.VMEM((4, NY, 2, 128), F32),
        pltpu.VMEM((4, 4, 16, 128), F32),
        pltpu.VMEM((4, 4, 16, 128), F32),
        pltpu.VMEM((4, 2, 128), F32),
        pltpu.VMEM((4, 4, 2, 128), F32),
        pltpu.VMEM((4, 16, 128), F32),
        pltpu.VMEM((4, 16, 128), F32),
        pltpu.VMEM((4, 4, 16, 128), F32),
        pltpu.VMEM((4, 4, 16, 128), F32),
        pltpu.VMEM((4, NY, 64, 128), BF16),
        pltpu.VMEM((4, NY, 64, 128), BF16),
        pltpu.VMEM((4, HALO, 128), BF16),
        pltpu.VMEM((4, HALO, 128), BF16),
        pltpu.VMEM((4, HALO + POS, 128), F32),
        pltpu.VMEM((4, POS, 128), F32),
        pltpu.VMEM((8, 128), F32),
        pltpu.VMEM((3, 8, 128), F32),
        pltpu.VMEM((3, POS, 128), BF16),
        pltpu.VMEM((4, POS, 128), BF16),
        pltpu.VMEM((3, POS, 256), BF16),
        pltpu.VMEM((4, POS, 256), BF16),
        dma((13,)),
        dma((5,)), dma((6,)),
        dma(()), dma((6,)),
        dma((2,)), dma((4, 2)),
        dma((2,)), dma((4, 2)),
        dma(()), dma((4,)),
        dma(()), dma((4,)),
        dma(()), dma((4,)),
        dma(()), dma((4,)),
        dma(()), dma(()),
        dma(()), dma(()),
        dma(()), dma((3,)),
        dma((2,)), dma((4, 2, 2)),
        dma((2,)), dma((2,)),
        pltpu.SemaphoreType.REGULAR, pltpu.SemaphoreType.REGULAR,
    ]
    anywhere = pl.BlockSpec(memory_space=pltpu.HBM)
    return pl.pallas_call(
        kernel,
        out_shape=jax.ShapeDtypeStruct((1, POS, D), BF16),
        in_specs=[anywhere] * 16,
        out_specs=pl.BlockSpec(memory_space=pltpu.VMEM),
        scratch_shapes=scratch,
        compiler_params=pltpu.CompilerParams(
            collective_id=0, has_side_effects=True, vmem_limit_bytes=67043328 - 270 * 1024
        ),
        name="mixer",
    )(
        frames, norm_gain.reshape(1, -1), conv_value_w.T, conv_gate_w.T, conv_taps,
        conv_bias.reshape(1, -1), channel_gain.reshape(1, -1), channel_shift.reshape(1, -1),
        query_w, forget_w, input_w, gate_w, memory_rate.reshape(1, -1), head_gain.reshape(1, -1),
        conv_out_w, rec_out_w,
    )


def solution(mesh):
    torus = Mesh(mesh.devices.reshape(NZ, NY, NX, 2), ("z", "y", "x", "c"))
    tp, sp = ("x", "c"), ("z", "y")
    columns, rows, vector = P(None, tp), P(tp, None), P(tp)
    in_specs = (
        P(tp, sp, None), P(), columns, columns, columns, vector, vector, vector,
        columns, columns, columns, columns, vector, vector, rows, rows,
    )
    return jax.shard_map(
        local, mesh=torus, in_specs=in_specs, out_specs=P(tp, sp, None), check_vma=False
    )
```

time: 63.2 us -> 43.1 us (0.68)
  Pallas kernels: 53.4 us -> 41.3 us
  local copies, waits for them, and re-layouts: 9.38 us -> 1.67 us
    pallas_call x1, Pallas kernels: 53.4 us -> 41.3 us  [local(): pl.pallas_call(kernel, out_shape=jax.ShapeDtypeStruct((1, POS, D), BF16),...]
    unnamed x31 -> x1, local copies, waits for them, and re-layouts: 9.38 us -> 1.67 us
where the time goes in v3:
time: 43.1 us; the launch traced here: 43 us
  Pallas kernels  41.3 us (96%)
  local copies, waits for them, and re-layouts  1.67 us (4%)
    pallas_call x1, Pallas kernels, local(): pl.pallas_call(kernel, out_shape=jax.ShapeDtypeStruct((1, POS, D), BF16),...  41.3 us
    unnamed x1, local copies, waits for them, and re-layouts  1.67 us

profile of v3, /device:TPU:224, one launch (start us, length us, event | category | flops | bytes accessed | tf_op | source)
XLA Modules:
  0.0 43.0 jit_solution(16904363229196360294)
XLA Ops:
  0.0 41.3 %mixer.1 = bf16[1,128,1024]{2,1,0:T(8,128)(2,1)} custom-call(bf16[1,128,1024]{2,1,0:T(8,128)(2,1)} %frames.1, f32[1,1024]{1,0:T(1,128)} %bitcast.10, bf16[64,1024]{1,0:T(8,128)(2,1)} %bitcast.8, bf16[64,1024]{1,0:T(8,128)(2,1)} %bitcast.9, bf16[31,64]{1,0:T(8,128)(2,1)} %taps.1, f32[1,64]{1,0:T(1,128)} %bitcast.11, f32[1,64]{1,0:T(1,128)} %bitcast.12, ...), custom_call_target="tpu_custom_call" | custom-call | tf_op jit(solution)/shard_map/mixer/pallas_call | solution.py:587
  41.3 1.7 %copy.18 = bf16[1,128,1024]{2,1,0:T(8,128)(2,1)} copy(bf16[1,128,1024]{2,1,0:T(8,128)(2,1)} %mixer.1) | data formatting | bytes 524288

commit v4 on v3

--- a/solution.py
+++ b/solution.py
@@ -40,14 +40,21 @@
     out,
     fr_v, ng_v, taps_v, vec_v, hv_v, pk, xs, w, cwt, wc, wr,
     grown_b, inp_b, gate_b, local_b, gt_b, cum_b,
-    st_s, st_r, dec_s, dec_r, t_s, t_r, dd_s, dd_r, u_s, u_r, e_s, e_r, c_s, c_r,
+    st_s, st_r, dec_s, dec_r, t_s, t_r, dd_s, dd_r, c_s, c_r,
     halo_s, halo_r, ext, filt, stat_s, stat_r, ac_s, ac_r, ar_s, ar_r,
-    lsem, psend, precv, gsend, grecv, r1s, r1r, r2s, r2r, x2s, x2r, h2s, h2r, r3s, r3r, hs, hr,
+    lsem, psend, precv, gsend, grecv, r1s, r1r, r2s, r2r, r3s, r3r, hs, hr,
     ss, sr, acs, acr, ars, arr, wxs, wxr, wfs, wfr, y_in, z_in,
 ):
     z, y, x, c = (lax.axis_index(a) for a in ("z", "y", "x", "c"))
     partner = {"c": 1 - c}
-    upper, deep = lax.div(z, 4), lax.rem(z, 4)
+    pair, odd = lax.div(z, 2), lax.rem(z, 2)
+    me = odd * NY + y
+
+    def mate(flip, k):
+        z2, y2 = lax.rem(odd + flip, 2), lax.rem(y + k, NY)
+        return {"z": 2 * pair + z2, "y": y2}, z2 * NY + y2
+
+    mates = [mate(*m) for m in ((1, 2), (1, 1), (1, 3), (1, 0), (0, 2), (0, 1), (0, 3))]
 
     def at_x(k):
         return {"x": lax.rem(x + k + NX, NX)}
@@ -66,15 +73,22 @@
     for k in (1, 2, 3):
         signal(bar, at_x(k))
 
-    @pl.loop(y + 1, NY)
+    def rank(number):
+        return 2 * lax.min(lax.rem(number, NY), 2) + 2 * lax.div(number, NY)
+
+    ahead = 0
+    for dev, number in mates:
+        ahead = ahead + jnp.where(rank(number) <= rank(me), 1, 0)
+
+        @pl.when(rank(number) >= rank(me))
+        def _():
+            signal(bar, dev)
+
+    @pl.loop(pair + 1, 4)
     def _(i):
-        signal(bar, {"y": i})
-
-    @pl.loop(z + 1, NZ)
-    def _(i):
-        signal(bar, {"z": i})
-
-    @pl.when((y == 0) & (z > 0))
+        signal(bar, {"z": 2 * i + odd})
+
+    @pl.when((y == 0) & (odd == 0) & (z > 0))
     def _():
         signal(bar, {"z": z - 1, "y": NY - 1})
 
@@ -116,7 +130,7 @@
 
     pl.semaphore_wait(
         bar,
-        4 + y + z + jnp.where((y == NY - 1) & (z < NZ - 1), 1, 0),
+        4 + ahead + pair + jnp.where((y == NY - 1) & (odd == 1) & (z < NZ - 1), 1, 0),
     )
 
     def half(ref, s, h):
@@ -133,17 +147,15 @@
     for copy in g[:4]:
         copy.start()
 
-    @pl.loop(0, y)
+    for dev, number in mates:
+
+        @pl.when(rank(number) < rank(me))
+        def _():
+            signal(y_in, dev)
+
+    @pl.loop(0, pair)
     def _(i):
-        signal(y_in, {"y": i})
-
-    @pl.loop(4 * upper, z)
-    def _(i):
-        signal(z_in, {"z": i})
-
-    @pl.when(upper == 1)
-    def _():
-        signal(z_in, {"z": z - 4})
+        signal(z_in, {"z": 2 * i + odd})
 
     remote(fw, w.at[:, pl.ds(FG + 128, 128)], psend.at[0], precv.at[0], partner).start()
     remote(iw, w.at[:, pl.ds(IN + 128, 128)], psend.at[0], precv.at[0], partner).start()
@@ -176,7 +188,7 @@
 
     def spread(rows2):
         return jnp.concatenate(
-            [jnp.broadcast_to(rows2[h : h + 1], (32, 128)) for h in range(2)], axis=0
+            [jnp.broadcast_to(rows2[h : h + 1], (16, 128)) for h in range(2)], axis=0
         )
 
     def begin(j):
@@ -197,20 +209,19 @@
             state = lax.dot_general(
                 inputs[:, lanes], weighted[:, lanes], TN, preferred_element_type=F32
             )
-            for k in range(NY):
-                st_s[j, k, 32 * h : 32 * h + 32] = state[32 * k : 32 * k + 32]
+            for k in range(8):
+                st_s[j, k, 16 * h : 16 * h + 16] = state[16 * k : 16 * k + 16]
             dec_s[j, h : h + 1] = jnp.exp(last[:, lanes])
         gt_b[j] = in_gate
         cum_b[j] = cumulative
         inp_b[j] = inputs
 
     def deal(j):
-        for k in (2, 1, 3):
-            to = lax.rem(y + k, NY)
-            remote(st_s.at[j, to], st_r.at[j, y], r1s.at[0], r1r.at[j, 0], {"y": to}).start()
-            remote(dec_s.at[j], dec_r.at[j, y], r1s.at[1], r1r.at[j, 1], {"y": to}).start()
-        st_r[j, y] = st_s[j, y]
-        dec_r[j, y] = dec_s[j]
+        for dev, to in mates:
+            remote(st_s.at[j, to], st_r.at[j, me], r1s.at[0], r1r.at[j, 0], dev).start()
+            remote(dec_s.at[j], dec_r.at[j, me], r1s.at[1], r1r.at[j, 1], dev).start()
+        st_r[j, me] = st_s[j, me]
+        dec_r[j, me] = dec_s[j]
 
     def gating(j):
         rows = xs[j]
@@ -248,62 +259,41 @@
         gate_b[j] = dot(rows, w[:, GA : GA + 256]).astype(BF16)
 
     def totals(j):
-        arrived(st_r.at[j, pl.ds(0, 3)], r1r.at[j, 0])
-        arrived(dec_r.at[j, pl.ds(0, 3)], r1r.at[j, 1])
+        arrived(st_r.at[j, pl.ds(0, 7)], r1r.at[j, 0])
+        arrived(dec_r.at[j, pl.ds(0, 7)], r1r.at[j, 1])
         total = st_r[j, 0]
         decay = dec_r[j, 0]
-        for k in (1, 2, 3):
+        for k in range(1, 8):
             total = total * spread(dec_r[j, k]) + st_r[j, k]
             decay = decay * dec_r[j, k]
-        t_s[j] = total.reshape(4, 16, 128)
+        t_s[j] = total
         dd_s[j] = decay
-        for k in (2, 1, 3):
-            to = lax.rem(deep + k, 4)
-            dev = {"z": 4 * upper + to}
-            remote(t_s.at[j, to], t_r.at[j, deep], r2s.at[0], r2r.at[j, 0], dev).start()
-            remote(dd_s.at[j], dd_r.at[j, deep], r2s.at[1], r2r.at[j, 1], dev).start()
-        t_r[j, deep] = t_s[j, deep]
-        dd_r[j, deep] = dd_s[j]
-
-    def fold(j):
-        head = lax.div(deep, 2)
-        arrived(t_r.at[j, pl.ds(0, 3)], r2r.at[j, 0])
-        arrived(dd_r.at[j, pl.ds(0, 3)], r2r.at[j, 1])
-
-        @pl.when(upper == 0)
-        def _():
-            u_r[j] = jnp.zeros((16, 128), F32)
-
-        @pl.when(upper == 1)
-        def _():
-            arrived(u_r.at[j], x2r.at[j])
-
-        state = u_r[j]
-        for i in range(4):
-            e_s[j, i] = state
-            state = state * dd_r[j, i, pl.ds(head, 1)] + t_r[j, i]
-        u_s[j] = state
-
-        @pl.when(upper == 0)
-        def _():
-            remote(u_s.at[j], u_r.at[j], x2s, x2r.at[j], {"z": z + 4}).start()
-
-        for k in (2, 1, 3):
-            to = lax.rem(deep + k, 4)
-            remote(e_s.at[j, to], e_r.at[j, deep], h2s, h2r.at[j], {"z": 4 * upper + to}).start()
-        e_r[j, deep] = e_s[j, deep]
+
+        @pl.loop(pair + 1, 4)
+        def _(i):
+            dev = {"z": 2 * i + odd}
+            remote(t_s.at[j], t_r.at[j, pair], r2s.at[0], r2r.at[j, 0], dev).start()
+            remote(dd_s.at[j], dd_r.at[j, pair], r2s.at[1], r2r.at[j, 1], dev).start()
 
     def carry(j):
-        arrived(e_r.at[j, pl.ds(0, 3)], h2r.at[j])
-        state = e_r[j].reshape(64, 128)
-        for k in range(NY):
+        for n in (1, 2, 3):
+
+            @pl.when(pair == n)
+            def _():
+                arrived(t_r.at[j, pl.ds(0, n)], r2r.at[j, 0])
+                arrived(dd_r.at[j, pl.ds(0, n)], r2r.at[j, 1])
+
+        def step(i, state):
+            return state * spread(dd_r[j, i]) + t_r[j, i]
+
+        state = lax.fori_loop(0, pair, step, jnp.zeros((32, 128), F32))
+        for k in range(8):
             c_s[j, k] = state.astype(BF16)
-            if k < NY - 1:
+            if k < 7:
                 state = state * spread(dec_r[j, k]) + st_r[j, k]
-        for k in (2, 1, 3):
-            to = lax.rem(y + k, NY)
-            remote(c_s.at[j, to], c_r.at[j, y], r3s, r3r.at[j], {"y": to}).start()
-        c_r[j, y] = c_s[j, y]
+        for dev, to in mates:
+            remote(c_s.at[j, to], c_r.at[j, me], r3s, r3r.at[j], dev).start()
+        c_r[j, me] = c_s[j, me]
 
     def filtering(j):
         @pl.when((z > 0) | (y > 0))
@@ -329,13 +319,13 @@
         return (scaled * sigmoid(scaled)).astype(BF16)
 
     def finish(j):
-        arrived(c_r.at[j, pl.ds(0, 3)], r3r.at[j])
+        arrived(c_r.at[j, pl.ds(0, 7)], r3r.at[j])
         gate = gate_b[j].astype(F32)
         silu = gate * sigmoid(gate)
         parts = []
         for h in range(2):
             lanes = slice(128 * h, 128 * h + 128)
-            low = jnp.concatenate([c_r[j, k, 32 * h : 32 * h + 32] for k in range(NY)], axis=0)
+            low = jnp.concatenate([c_r[j, k, 16 * h : 16 * h + 16] for k in range(8)], axis=0)
             raw = local_b[j, :, lanes] + lax.dot_general(
                 grown_b[j, :, lanes], low, NT, preferred_element_type=F32
             )
@@ -385,15 +375,16 @@
     begin(0)
     arrived(cwt.at[0], precv.at[2])
     gating(0)
-
-    @pl.when(y < NY - 1)
+    arrived(w.at[:, pl.ds(0, 256)], precv.at[1])
+    within(0)
+    behind = 7 - ahead
+
+    @pl.when(behind > 0)
     def _():
-        pl.semaphore_wait(y_in, NY - 1 - y)
+        pl.semaphore_wait(y_in, behind)
 
     deal(0)
     pass_on(0)
-    arrived(w.at[:, pl.ds(0, 256)], precv.at[1])
-    within(0)
     g[0].wait_recv()
     g[4].start()
     g[1].wait_recv()
@@ -409,9 +400,9 @@
     begin(2)
     deal(2)
 
-    @pl.when(z < NZ - 1)
+    @pl.when(pair < 3)
     def _():
-        pl.semaphore_wait(z_in, 4 - deep - upper)
+        pl.semaphore_wait(z_in, 3 - pair)
 
     totals(0)
     g[4].wait_recv()
@@ -424,12 +415,15 @@
     pass_on(2)
     gating(3)
     pass_on(3)
+    within(1)
     totals(1)
     totals(2)
-    fold(0)
-    within(1)
+    carry(0)
+    within(2)
+    within(3)
+    sums = [filtering(j) for j in range(3)]
     totals(3)
-    sums = [filtering(j) for j in range(4)]
+    sums.append(filtering(3))
     lane = lax.broadcasted_iota(jnp.int32, (POS, 128), 1)
     packed = jnp.zeros((POS, 128), F32)
     for j in range(4):
@@ -438,14 +432,12 @@
     stat_s[...] = packed.T[0:8]
     for k in (1, -1, 2):
         remote(stat_s, stat_r.at[SLOT_OF[-k % NX] - 1], ss, sr, at_x(k)).start()
-    within(2)
-    fold(1)
-    fold(2)
     send_on(1, 0)
     send_on(-1, 1)
-    within(3)
-    carry(0)
-    fold(3)
+    carry(1)
+    carry(2)
+    spread_out(0, finish(0))
+    carry(3)
     arrived(stat_r, sr)
     total = stat_s[...]
     for s in (1, 2, 3):
@@ -462,12 +454,8 @@
         else:
             ac_s[j - 1] = rows
             remote(ac_s.at[j - 1], ac_r.at[SLOT_OF[-OFF[j] % NX] - 1], acs, acr, at_x(OFF[j])).start()
-    carry(1)
-    carry(2)
     over(1, (1,))
     over(2, (0,))
-    carry(3)
-    spread_out(0, finish(0))
     for j in (1, 2):
         rows = finish(j)
         spread_out(j, rows)
@@ -495,17 +483,16 @@
     sent(wc.at[0, pl.ds(0, 64)], psend.at[3])
     sent(wr.at[0, pl.ds(0, 128)], psend.at[4])
     sent(xs.at[pl.ds(0, 3)], gsend)
-    sent(st_s.at[pl.ds(0, 3)], r1s.at[0])
-    sent(dec_r.at[pl.ds(0, 3)], r1s.at[1])
-    sent(t_r.at[pl.ds(0, 3)], r2s.at[0])
-    sent(dd_r.at[pl.ds(0, 3)], r2s.at[1])
-    sent(e_r.at[pl.ds(0, 3)], h2s)
-
-    @pl.when(upper == 0)
-    def _():
-        sent(u_s, x2s)
-
-    sent(c_r.at[pl.ds(0, 3)], r3s)
+    sent(st_s.at[:, pl.ds(0, 7)], r1s.at[0])
+    sent(dec_r.at[:, pl.ds(0, 7)], r1s.at[1])
+    for n in (1, 2, 3):
+
+        @pl.when(pair == 3 - n)
+        def _():
+            sent(t_r.at[pl.ds(0, n)], r2s.at[0])
+            sent(dd_r.at[pl.ds(0, n)], r2s.at[1])
+
+    sent(c_r.at[:, pl.ds(0, 7)], r3s)
 
     @pl.when((y < NY - 1) | (z < NZ - 1))
     def _():
@@ -543,20 +530,16 @@
         pltpu.VMEM((4, POS, 256), F32),
         pltpu.VMEM((4, POS, 256), F32),
         pltpu.VMEM((4, POS, 256), F32),
-        pltpu.VMEM((4, NY, 64, 128), F32),
-        pltpu.VMEM((4, NY, 64, 128), F32),
+        pltpu.VMEM((4, 8, 32, 128), F32),
+        pltpu.VMEM((4, 8, 32, 128), F32),
         pltpu.VMEM((4, 2, 128), F32),
-        pltpu.VMEM((4, NY, 2, 128), F32),
-        pltpu.VMEM((4, 4, 16, 128), F32),
-        pltpu.VMEM((4, 4, 16, 128), F32),
+        pltpu.VMEM((4, 8, 2, 128), F32),
+        pltpu.VMEM((4, 32, 128), F32),
+        pltpu.VMEM((4, 4, 32, 128), F32),
         pltpu.VMEM((4, 2, 128), F32),
         pltpu.VMEM((4, 4, 2, 128), F32),
-        pltpu.VMEM((4, 16, 128), F32),
-        pltpu.VMEM((4, 16, 128), F32),
-        pltpu.VMEM((4, 4, 16, 128), F32),
-        pltpu.VMEM((4, 4, 16, 128), F32),
-        pltpu.VMEM((4, NY, 64, 128), BF16),
-        pltpu.VMEM((4, NY, 64, 128), BF16),
+        pltpu.VMEM((4, 8, 32, 128), BF16),
+        pltpu.VMEM((4, 8, 32, 128), BF16),
         pltpu.VMEM((4, HALO, 128), BF16),
         pltpu.VMEM((4, HALO, 128), BF16),
         pltpu.VMEM((4, HALO + POS, 128), F32),
@@ -574,8 +557,6 @@
         dma((2,)), dma((4, 2)),
         dma(()), dma((4,)),
         dma(()), dma((4,)),
-        dma(()), dma((4,)),
-        dma(()), dma((4,)),
         dma(()), dma(()),
         dma(()), dma(()),
         dma(()), dma((3,)),
@@ -591,15 +572,15 @@
         out_specs=pl.BlockSpec(memory_space=pltpu.VMEM),
         scratch_shapes=scratch,
         compiler_params=pltpu.CompilerParams(
-            collective_id=0, has_side_effects=True, vmem_limit_bytes=67043328 - 270 * 1024
+            collective_id=0, has_side_effects=True, vmem_limit_bytes=24 * 1024 * 1024
         ),
         name="mixer",
-    )(
+    )(*[pltpu.with_memory_space_constraint(a, pltpu.HBM) for a in (
         frames, norm_gain.reshape(1, -1), conv_value_w.T, conv_gate_w.T, conv_taps,
         conv_bias.reshape(1, -1), channel_gain.reshape(1, -1), channel_shift.reshape(1, -1),
         query_w, forget_w, input_w, gate_w, memory_rate.reshape(1, -1), head_gain.reshape(1, -1),
         conv_out_w, rec_out_w,
-    )
+    )])
 
 
 def solution(mesh):

time: 43.1 us -> 37.2 us (0.86)
  the two profiles are of different devices: /device:TPU:224 before, /device:TPU:102 now
where the time goes in v4:
time: 37.2 us; the launch traced here: 37.1 us
  Pallas kernels  36.3 us (98%)
  local copies, waits for them, and re-layouts  0.71 us (2%)
    pallas_call x1, Pallas kernels, local(): pl.pallas_call(kernel, out_shape=jax.ShapeDtypeStruct((1, POS, D), BF16),...  36.3 us

profile of v4, /device:TPU:102, one launch (start us, length us, event | category | flops | bytes accessed | tf_op | source)
XLA Modules:
  0.0 37.1 jit_solution(344025308486895923)
XLA Ops:
  0.0 36.3 %mixer.1 = bf16[1,128,1024]{2,1,0:T(8,128)(2,1)S(1)} custom-call(bf16[1,128,1024]{2,1,0:T(8,128)(2,1)} %frames.1, f32[1,1024]{1,0:T(1,128)} %bitcast.10, bf16[64,1024]{1,0:T(8,128)(2,1)} %bitcast.8, bf16[64,1024]{1,0:T(8,128)(2,1)} %bitcast.9, bf16[31,64]{1,0:T(8,128)(2,1)} %taps.1, f32[1,64]{1,0:T(1,128)} %bitcast.11, f32[1,64]{1,0:T(1,128)} %bitcast.12, ...), custom_call_target="tpu_custom_call" | custom-call | tf_op jit(solution)/shard_map/mixer/pallas_call | solution.py:568
  36.3 0.7 %copy.18 = bf16[1,128,1024]{2,1,0:T(8,128)(2,1)} copy(bf16[1,128,1024]{2,1,0:T(8,128)(2,1)S(1)} %mixer.1) | data formatting | bytes 524288
